TPU v7x, 512 devices: a whole 4x4x16 slice. The times are simulated.
512 devices in a mesh: sp: 64 (over z, y), tp: 8 (over x, core).
Axes of the slice: x: 4, y: 4, z: 16, core: 2. Of those that a mesh axis runs over, the one named last changes fastest.
Arguments:
- tokens: bfloat16 [16384, 2048], P('sp', 'tp'), may hold values from -6 to 6
- norm_gain: float32 [2048], replicated, may hold values from 0.1 to 1.9
- glu_value: bfloat16 [2048, 2048], P('sp', 'tp'), may hold values from -0.125 to 0.125
- glu_gate: bfloat16 [2048, 2048], P('sp', 'tp'), may hold values from -0.125 to 0.125
- conv_taps: float32 [31, 2048], P(None, 'tp'), may hold values from -11 to 11
- ln_gain: float32 [2048], P('tp'), may hold values from 0.1 to 1.9
- ln_bias: float32 [2048], P('tp'), may hold values from -3 to 3
- query_weight: bfloat16 [2048, 2048], P('sp', 'tp'), may hold values from -0.125 to 0.125
- key_weight: bfloat16 [2048, 2048], P('sp', 'tp'), may hold values from -0.125 to 0.125
- value_weight: bfloat16 [2048, 2048], P('sp', 'tp'), may hold values from -0.125 to 0.125
- gate_weight: bfloat16 [2048, 32], replicated, may hold values from -0.125 to 0.125
- gate_bias: float32 [32], replicated, may hold values from -1 to 110
- log_decay_extra: float32 [16384, 16], P('sp'), may hold values from -1.3 to 0
- mem_gain: float32 [2048], P('tp'), may hold values from 0.1 to 1.9
- out_conv: bfloat16 [2048, 2048], P('tp'), may hold values from -0.125 to 0.125
- out_mem: bfloat16 [2048, 2048], P('tp'), may hold values from -0.125 to 0.125
Outputs:
- mixed: bfloat16 [16384, 2048], P(('sp', 'tp'))
All inputs are finite; a program needn't handle non-finite values.
Results may differ from a plain program's by a relative error of at most 0.015.
Values may be sent and summed in bfloat16 or wider, within the bound.
A program may use at most 128 MiB of HBM per device.

v0:
```python
import jax
import jax.numpy as jnp
from jax import lax
from jax.sharding import Mesh
from jax.sharding import PartitionSpec as P

CONV = 2048
MEMORY_HEADS = 8
HEAD = 256
KW = 31
BLOCK = 128
SP = ("sp_0", "sp_1")
SP_TP = ("sp_0", "sp_1", "tp")


EPS = 1e-06
LOW_START = -1e30
PRECISE = lax.Precision.HIGHEST


def sent_to_all(array, axis):
    copies = jnp.broadcast_to(array, (lax.axis_size(axis), *array.shape))
    return lax.all_to_all(copies, axis, split_axis=0, concat_axis=0, tiled=True)


def joined_along(blocks, dim):
    shape = list(blocks.shape[1:])
    shape[dim] *= blocks.shape[0]
    return jnp.moveaxis(blocks, 0, dim).reshape(shape)


def collect(array, axis, dim):
    blocks = sent_to_all(array, axis)
    return joined_along(blocks, dim)


def extended(cells, sides, width):
    for axis, dim in sides:
        count = lax.axis_size(axis)
        ends = count - 1
        head = lax.slice_in_dim(cells, 0, width, axis=dim)
        tail = lax.slice_in_dim(cells, cells.shape[dim] - width, cells.shape[dim], axis=dim)
        cells = jnp.concatenate(
            [
                lax.ppermute(tail, axis, [(i, (i + 1) % count) for i in range(ends)]),
                cells,
                lax.ppermute(head, axis, [((i + 1) % count, i) for i in range(ends)]),
            ],
            axis=dim,
        )
    return cells


def of_everyone(array, axis):
    return sent_to_all(array, axis).sum(axis=0)


def together(arrays, axis):
    ends = [0]
    for a in arrays:
        ends.append(ends[-1] + a.size)
    total = of_everyone(jnp.concatenate([a.ravel() for a in arrays]), axis)
    return tuple((total[b:e].reshape(a.shape) for a, b, e in zip(arrays, ends, ends[1:])))


def nothing_yet(array, identity):
    return jax.tree.map(
        lambda a, e: jnp.broadcast_to(jnp.asarray(e, a.dtype), a.shape), array, identity
    )


def prefix_by_axis(array, axes, combine, identity):
    before = start = nothing_yet(array, identity)
    total = array
    for axis in reversed(axes):
        length, place = (lax.axis_size(axis), lax.axis_index(axis))
        pieces = jax.tree.map(lambda part: lax.all_gather(part, axis), total)
        inside, total = (start, start)
        for k in range(length):
            passed = k < place
            total = combine(total, jax.tree.map(lambda part: part[k], pieces))
            inside = jax.tree.map(lambda new, old: jnp.where(passed, new, old), total, inside)
        before = combine(inside, before)
    return before


def gathered_once(array, axis):
    leaves = jax.tree.leaves(array)
    order = sorted(range(len(leaves)), key=lambda k: -leaves[k].size)
    width = (1, *leaves[order[0]].shape)[-1]
    lines = [
        jnp.pad(leaves[k].reshape(-1), (0, -leaves[k].size % width)).reshape(-1, width)
        for k in order
    ]
    both, at, found = (lax.all_gather(jnp.concatenate(lines), axis), 0, {})
    for k, line in zip(order, lines):
        section = both[:, at : at + len(line)].reshape(len(both), -1)
        found[k] = section[:, : leaves[k].size].reshape(-1, *leaves[k].shape)
        at += len(line)
    numbers = iter(range(len(leaves)))
    return jax.tree.map(lambda _: found[next(numbers)], array)


def entering(array, axes, combine, identity):
    before = start = nothing_yet(array, identity)
    total = array
    for axis in reversed(axes):
        length, place = (lax.axis_size(axis), lax.axis_index(axis))
        pieces = gathered_once(total, axis)
        inside, total = (start, start)
        for k in reversed(range(length)):
            passed = k > place
            total = combine(total, jax.tree.map(lambda part: part[k], pieces))
            inside = jax.tree.map(lambda new, old: jnp.where(passed, new, old), total, inside)
        before = combine(inside, before)
    return before


def sent_together(arrays, axis, dim, along):
    widths = [a.shape[along] for a in arrays]
    both = jnp.concatenate(arrays, axis=along)
    filled = lax.all_gather(both, axis, axis=dim, tiled=True)
    return tuple(jnp.split(filled, [sum(widths[:k]) for k in range(1, len(widths))], axis=along))


def split_up(array, dim, length):
    shape = array.shape
    blocks = array.reshape(*shape[:dim], length, shape[dim] // length, *shape[dim + 1 :])
    return jnp.moveaxis(blocks, dim, 0)


def sent_and_summed(array, axis, dim):
    length = lax.axis_size(axis)
    blocks = lax.all_to_all(split_up(array, dim, length), axis, 0, 0, tiled=True)
    return jnp.sum(blocks.astype(jnp.float32), axis=0)


def block_step(carried_state, block_data):
    state_mat, state_vec, stabilizer = carried_state
    queries, key_rows, value_rows, input_gate, log_forget = block_data
    key_scale = HEAD ** (-0.5)
    length = log_forget.shape[-1]
    causal = jnp.tril(jnp.ones((length, length), dtype=bool))
    decay_sum = jnp.cumsum(log_forget, axis=-1)
    log_weight = jnp.where(
        causal, decay_sum[:, :, None] - decay_sum[:, None, :] + input_gate[:, None, :], -jnp.inf
    )
    carried = decay_sum + stabilizer[:, None]
    running = jnp.maximum(carried, jnp.max(log_weight, axis=-1))
    inner_weight = jnp.exp(log_weight - running[:, :, None])
    carry_weight = jnp.exp(carried - running)
    raw_scores = jnp.einsum("htd,hsd->hts", queries, key_rows, preferred_element_type=jnp.float32)
    scores = raw_scores * key_scale * inner_weight
    query_wide = queries.astype(jnp.float32)
    numerator = carry_weight[:, :, None] * jnp.einsum(
        "htd,hde->hte", query_wide, state_mat, precision=PRECISE
    )
    numerator = numerator + jnp.einsum(
        "hts,hse->hte", scores.astype(jnp.bfloat16), value_rows, preferred_element_type=jnp.float32
    )
    denominator = carry_weight * jnp.einsum(
        "htd,hd->ht", query_wide, state_vec, precision=PRECISE
    ) + jnp.sum(scores, axis=-1)
    to_end = decay_sum[:, -1:] - decay_sum + input_gate
    carried_end = decay_sum[:, -1] + stabilizer
    new_stabilizer = jnp.maximum(carried_end, jnp.max(to_end, axis=-1))
    end_weight = jnp.exp(to_end - new_stabilizer[:, None]) * key_scale
    keep_weight = jnp.exp(carried_end - new_stabilizer)
    weighted = key_rows.astype(jnp.float32) * end_weight[:, :, None]
    new_mat = keep_weight[:, None, None] * state_mat + jnp.einsum(
        "hsd,hse->hde",
        weighted.astype(jnp.bfloat16),
        value_rows,
        preferred_element_type=jnp.float32,
    )
    new_vec = keep_weight[:, None] * state_vec + jnp.sum(weighted, axis=1)
    return ((new_mat, new_vec, new_stabilizer), (numerator, denominator, running, decay_sum))


def local_pass(queries, key_rows, value_rows, input_gate, log_forget):
    head_count, length, head_width = queries.shape
    count = length // BLOCK

    def blocked(tensor):
        return jnp.moveaxis(tensor.reshape((head_count, count, BLOCK) + tensor.shape[2:]), 1, 0)

    def unblocked(tensor):
        return jnp.moveaxis(tensor, 0, 1).reshape((head_count, length) + tensor.shape[3:])

    start = (
        jnp.zeros((head_count, head_width, head_width), jnp.float32),
        jnp.zeros((head_count, head_width), jnp.float32),
        jnp.full((head_count,), LOW_START, jnp.float32),
    )
    final, outputs = lax.scan(
        block_step,
        start,
        (
            blocked(queries),
            blocked(key_rows),
            blocked(value_rows),
            blocked(input_gate),
            blocked(log_forget),
        ),
    )
    numerator, denominator, running, decay_sum = outputs
    totals = decay_sum[:, :, -1]
    offsets = jnp.cumsum(totals, axis=0) - totals
    decay_sum = decay_sum + offsets[:, :, None]
    summary = (offsets[-1] + totals[-1], final[0], final[1], final[2])
    return (
        unblocked(numerator),
        unblocked(denominator),
        unblocked(running),
        unblocked(decay_sum),
        summary,
    )


def compose(earlier, later):
    early_decay, early_mat, early_vec, early_level = earlier
    late_decay, late_mat, late_vec, late_level = later
    stabilizer = jnp.maximum(early_level + late_decay, late_level)
    early_weight = jnp.exp(early_level + late_decay - stabilizer)
    late_weight = jnp.exp(late_level - stabilizer)
    return (
        early_decay + late_decay,
        early_weight[:, None, None] * early_mat + late_weight[:, None, None] * late_mat,
        early_weight[:, None] * early_vec + late_weight[:, None] * late_vec,
        stabilizer,
    )


def finish(queries, numerator, denominator, running, decay_sum, incoming):
    in_mat, in_vec, in_level = (incoming[1], incoming[2], incoming[3])
    query_wide = queries.astype(jnp.float32)
    carried = decay_sum + in_level[:, None]
    stabilizer = jnp.maximum(running, carried)
    local_weight = jnp.exp(running - stabilizer)
    carry_weight = jnp.exp(carried - stabilizer)
    numerator = local_weight[:, :, None] * numerator
    numerator = numerator + carry_weight[:, :, None] * jnp.einsum(
        "htd,hde->hte", query_wide, in_mat, precision=PRECISE
    )
    denominator = local_weight * denominator + carry_weight * jnp.einsum(
        "htd,hd->ht", query_wide, in_vec, precision=PRECISE
    )
    return numerator / jnp.maximum(jnp.abs(denominator), jnp.exp(-stabilizer))[:, :, None]


def shards(
    tokens,
    norm_gain,
    glu_value,
    glu_gate,
    conv_taps,
    ln_gain,
    ln_bias,
    query_weight,
    key_weight,
    value_weight,
    gate_weight,
    gate_bias,
    log_decay_extra,
    mem_gain,
    out_conv,
    out_mem,
):
    whole_rows = collect(tokens, "tp", 1)
    wide = whole_rows.astype(jnp.float32)
    normed = (
        wide * lax.rsqrt(jnp.mean(wide * wide, axis=-1, keepdims=True) + EPS) * norm_gain
    ).astype(jnp.bfloat16)
    row_count = normed.shape[0]
    head_count = mem_gain.shape[0] // HEAD
    first_head = lax.axis_index("tp") * head_count
    gate_all = (
        jnp.dot(normed, gate_weight, preferred_element_type=jnp.float32) + gate_bias
    ).reshape(row_count, 4, MEMORY_HEADS)
    own_gates = lax.dynamic_slice_in_dim(gate_all, first_head, head_count, 2)
    own_extra = lax.dynamic_slice_in_dim(
        log_decay_extra.reshape(row_count, 2, MEMORY_HEADS), first_head, head_count, 2
    )

    def memory_branch(query_proj, key_proj, value_proj):

        def head_major(tensor):
            return jnp.transpose(tensor.reshape(row_count, head_count, HEAD), (1, 0, 2))

        queries = head_major(query_proj)
        key_rows = head_major(key_proj)
        value_rows = head_major(value_proj)
        input_fwd = own_gates[:, 0, :].T
        forget_fwd = (jax.nn.log_sigmoid(own_gates[:, 1, :]) + own_extra[:, 0, :]).T
        input_bwd = own_gates[:, 2, :].T
        forget_bwd = (jax.nn.log_sigmoid(own_gates[:, 3, :]) + own_extra[:, 1, :]).T
        identity = (
            jnp.zeros((head_count,), jnp.float32),
            jnp.zeros((head_count, HEAD, HEAD), jnp.float32),
            jnp.zeros((head_count, HEAD), jnp.float32),
            jnp.full((head_count,), LOW_START, jnp.float32),
        )
        numerator, denominator, running, decay_sum, summary = local_pass(
            queries, key_rows, value_rows, input_fwd, forget_fwd
        )
        incoming = prefix_by_axis(summary, SP, compose, identity)
        forward_out = finish(queries, numerator, denominator, running, decay_sum, incoming)
        back_queries = jnp.flip(queries, 1)
        numerator, denominator, running, decay_sum, summary = local_pass(
            back_queries,
            jnp.flip(key_rows, 1),
            jnp.flip(value_rows, 1),
            jnp.flip(input_bwd, 1),
            jnp.flip(forget_bwd, 1),
        )
        incoming = entering(summary, SP, compose, identity)
        backward_out = jnp.flip(
            finish(back_queries, numerator, denominator, running, decay_sum, incoming), 1
        )
        summed = forward_out + backward_out
        head_norm = summed * lax.rsqrt(jnp.mean(summed * summed, axis=-1, keepdims=True) + EPS)
        head_norm = head_norm * mem_gain.reshape(head_count, HEAD)[:, None, :]
        return (
            jnp.transpose(head_norm, (1, 0, 2))
            .reshape(row_count, head_count * HEAD)
            .astype(jnp.bfloat16)
        )

    pieces = sent_together((glu_value, glu_gate, query_weight, key_weight, value_weight), SP, 0, 1)
    sums = tuple(
        (jnp.dot(normed, weight_rows, preferred_element_type=jnp.float32) for weight_rows in pieces)
    )
    glu = (sums[0] * jax.nn.sigmoid(sums[1])).astype(jnp.bfloat16)
    projected = tuple((each_sum.astype(jnp.bfloat16) for each_sum in sums[2:]))
    reach = KW // 2
    padded = extended(glu, ((SP, 0),), reach).astype(jnp.float32)
    conv = jnp.zeros(glu.shape, jnp.float32)
    for offset in range(KW):
        conv = conv + conv_taps[offset] * padded[offset : offset + row_count]
    chan_sums = jnp.sum(conv, axis=-1)
    chan_squares = jnp.sum(conv * conv, axis=-1)
    chan_sums, chan_squares = together((chan_sums, chan_squares), "tp")
    chan_mean = chan_sums / CONV
    chan_var = chan_squares / CONV - chan_mean * chan_mean
    normal = (conv - chan_mean[:, None]) * lax.rsqrt(chan_var + EPS)[:, None] * ln_gain + ln_bias
    act = (normal * jax.nn.sigmoid(normal)).astype(jnp.bfloat16)
    memory = memory_branch(*projected)
    result = jnp.dot(act, out_conv, preferred_element_type=jnp.float32)
    mixed = sent_and_summed(
        (result + jnp.dot(memory, out_mem, preferred_element_type=jnp.float32)).astype(
            jnp.bfloat16
        ),
        "tp",
        0,
    )
    return mixed.astype(jnp.bfloat16)


def solution(mesh):
    split = Mesh(mesh.devices.reshape(16, 4, mesh.shape["tp"]), ("sp_0", "sp_1", "tp"))
    placed = (
        P(SP, "tp"),
        P(),
        P(SP, "tp"),
        P(SP, "tp"),
        P(None, "tp"),
        P("tp"),
        P("tp"),
        P(SP, "tp"),
        P(SP, "tp"),
        P(SP, "tp"),
        P(),
        P(),
        P(SP, None),
        P("tp"),
        P("tp", None),
        P("tp", None),
    )
    return jax.shard_map(
        shards, mesh=split, in_specs=placed, out_specs=P(SP_TP, None), check_vma=False
    )
```

profile of v0, /device:TPU:1, one launch (start us, length us, event | category | flops | bytes accessed | tf_op | source)
XLA Modules:
  0.0 481.3 jit_solution(11081831425046455512)
XLA Ops:
  13.0 10.3 %all-to-all-start = ((bf16[8,256,256]{1,2,0:T(8,128)(2,1)}), bf16[8,256,256]{1,2,0:T(8,128)(2,1)S(1)}, u32[]{:S(2)}, u32[]{:S(2)}) async-start(bf16[8,256,256]{1,2,0:T(8,128)(2,1)} %broadcast_in_dim.45), calls=%async_computation | async-start | bytes 2097152 | tf_op jit(solution)/shard_map/all_to_all | solution.py:23
  23.3 15.0 %all-to-all-done = bf16[8,256,256]{1,2,0:T(8,128)(2,1)S(1)} async-done(((bf16[8,256,256]{1,2,0:T(8,128)(2,1)}), bf16[8,256,256]{1,2,0:T(8,128)(2,1)S(1)}, u32[]{:S(2)}, u32[]{:S(2)}) %all-to-all-start) | async-done | bytes 1048608 | tf_op jit(solution)/shard_map/all_to_all | solution.py:23
  39.3 1.6 fusion.96
  45.2 110.8 %all-gather.17.cloned.1.call-done = bf16[2048,1280]{1,0:T(8,128)(2,1)} async-done(((bf16[32,1280]{1,0:T(8,128)(2,1)}), bf16[2048,1280]{1,0:T(8,128)(2,1)}) %all-gather.17.cloned.1.call-update) | async-done | bytes 5242896 | tf_op jit(solution)/shard_map/all_gather | solution.py:122
  155.9 1.7 convolution_convert_fusion
  157.8 1.7 convolution_convert_fusion.2
  159.7 1.7 convolution_convert_fusion.1
  164.1 25.6 %while.47 = (s32[]{:T(128)}, f32[1,256,256]{2,1,0:T(8,128)S(1)}, f32[1,256]{1,0:T(1,128)S(1)}, f32[1]{0:T(128)}, f32[2,1,128,256]{3,2,1,0:T(8,128)}, /*index=5*/...) while((s32[]{:T(128)}, f32[1,256,256]{2,1,0:T(8,128)S(1)}, ...), condition=%wide.region_18.19_spmd.clone, body=%wide.region_12.18_spmd.clone.sunk | while | flops 135383168 | bytes 1799479 | solution.py:195
  166.3 1.9 fusion.751
  168.8 1.8 exponential_multiply_fusion.5
  173.6 1.4 fusion.758
  179.1 1.9 fusion.751
  181.6 1.8 exponential_multiply_fusion.5
  194.8 15.5 %while.46 = (s32[]{:T(128)}, f32[1,256,256]{2,1,0:T(8,128)S(1)}, f32[1,256]{1,0:T(1,128)S(1)}, f32[1]{0:T(128)}, f32[2,1,128,256]{3,2,1,0:T(8,128)S(1)}, /*index...) while((s32[]{:T(128)}, f32[1,256,256]{2,1,0:T(8,128)S(1)}, ...), condition=%wide.region_10.11_spmd.clone, body=%wide.region_4.10_spmd.clone.sunk | while | flops 135383168 | bytes 1796895 | solution.py:195
  197.0 2.0 fusion.734
  204.7 2.0 fusion.734
  211.0 17.4 %all-gather.23.cloned.1.call-done = f32[4,259,256]{2,1,0:T(8,128)} async-done(((f32[1,259,256]{2,1,0:T(8,128)}), f32[4,259,256]{2,1,0:T(8,128)}) %all-gather.23.cloned.1.call-update) | async-done | bytes 1060880 | tf_op jit(solution)/shard_map/all_gather | solution.py:95
  247.9 2.1 fusion.568
  250.0 8.0 %all-reduce.9 = (f32[4]{0:T(128)S(1)}, f32[4]{0:T(128)S(1)}) all-reduce(f32[4]{0:T(128)S(1)} %dynamic-update-slice.2, f32[4]{0:T(128)S(1)} %fusion.568), channel_id=4, replica_groups=mesh['sp_0'=16,'sp_1'=4,'tp'=8] {'sp_1'}, use_global_device_ids=true, to_apply=%add.6 | all-reduce | flops 8 | bytes 64
  271.6 2.0 fusion.161
  280.7 27.7 %all-reduce.8 = (f32[16]{0:T(128)S(1)}, f32[16]{0:T(128)S(1)}) all-reduce(f32[16]{0:T(128)S(1)} %dynamic-update-slice.1, f32[16]{0:T(128)S(1)} %dynamic-update-slice.3), channel_id=3, replica_groups=mesh['sp_0'=16,'sp_1'=4,'tp'=8] {'sp_0'}, use_global_device_ids=true, to_apply=%add.5 | all-reduce | flops 32 | bytes 256
  341.7 1.7 fusion.112
  343.4 1.7 fusion.106
  346.5 4.0 collective-permute-start
  352.1 6.0 %all-gather.8 = f32[4,1,256]{2,1,0:T(1,128)S(1)} all-gather(f32[1,1,256]{2,1,0:T(1,128)S(1)} %bitcast.725), channel_id=7, replica_groups=mesh['sp_0'=16,'sp_1'=4,'tp'=8] {'sp_1'}, dimensions={0}, use_global_device_ids=true | all-gather | bytes 5120 | tf_op jit(solution)/shard_map/all_gather | solution.py:77
  358.1 24.2 %all_gather.73 = f32[16,1,256]{2,1,0:T(1,128)S(1)} all-gather(f32[1,1,256]{2,1,0:T(1,128)S(1)} %get-tuple-element.441), channel_id=1, replica_groups=mesh['sp_0'=16,'sp_1'=4,'tp'=8] {'sp_0'}, dimensions={0}, use_global_device_ids=true | all-gather | bytes 17408 | tf_op jit(solution)/shard_map/all_gather | solution.py:77
  384.5 20.0 %all-to-all-start.1 = ((f32[8,1,512]{2,1,0:T(1,128)}), f32[8,1,512]{2,1,0:T(1,128)S(1)}, u32[]{:S(2)}, u32[]{:S(2)}) async-start(f32[8,1,512]{2,1,0:T(1,128)} %broadcast_in_dim.46), calls=%async_computation.1 | async-start | bytes 32768 | tf_op jit(solution)/shard_map/all_to_all | solution.py:23
  404.8 4.4 all-to-all-done.1
  409.3 1.9 fusion.303
  446.8 4.1 fusion.100
  451.4 3.8 multiply_reduce_fusion.1
  455.9 18.1 %all_to_all.16 = bf16[8,32,2048]{2,1,0:T(8,128)(2,1)S(1)} all-to-all(bf16[8,32,2048]{2,1,0:T(8,128)(2,1)S(1)} %bitcast.718), channel_id=1, replica_groups=mesh['sp_0'=16,'sp_1'=4,'tp'=8] {'tp'}, dimensions={0} | all-to-all | bytes 2097152 | tf_op jit(solution)/shard_map/all_to_all | solution.py:134
  (218 shorter events, 67.9 us)
Async XLA Ops:
  6.5 402.7 %copy-start = (bf16[256,2048]{1,0:T(8,128)(2,1)S(1)}, bf16[256,2048]{1,0:T(8,128)(2,1)}, u32[]{:S(2)}) copy-start(bf16[256,2048]{1,0:T(8,128)(2,1)} %param.34) | copy-start | bytes 3145732
  6.5 32.7 %copy-start.11 = (f32[2048]{0:T(1024)S(1)}, f32[2048]{0:T(1024)}, u32[]{:S(2)}) copy-start(f32[2048]{0:T(1024)} %param.21) | copy-start | bytes 24580
  6.5 34.3 %copy-start.7 = (bf16[2048,32]{0,1:T(8,128)(2,1)S(1)}, bf16[2048,32]{0,1:T(8,128)(2,1)}, u32[]{:S(2)}) copy-start(bf16[2048,32]{0,1:T(8,128)(2,1)} %param.30) | copy-start | bytes 393220
  6.5 34.3 %copy-start.22 = (f32[32]{0:T(128)S(1)}, f32[32]{0:T(128)}, u32[]{:S(2)}) copy-start(f32[32]{0:T(128)} %param.31) | copy-start | bytes 388
  6.5 149.4 %all-gather.17.cloned.1.call-start = ((), (), s32[]{:S(2)}) async-start(), calls=%async_computation.3 | async-start | bytes 5324800 | tf_op jit(solution)/shard_map/all_gather | solution.py:122
  13.0 25.3 %all-to-all-start = ((bf16[8,256,256]{1,2,0:T(8,128)(2,1)}), bf16[8,256,256]{1,2,0:T(8,128)(2,1)S(1)}, u32[]{:S(2)}, u32[]{:S(2)}) async-start(bf16[8,256,256]{1,2,0:T(8,128)(2,1)} %broadcast_in_dim.45), calls=%async_computation | async-start | bytes 2097152 | tf_op jit(solution)/shard_map/all_to_all | solution.py:23
  23.3 205.2 %all-gather.23.cloned.1.call-start = ((), (), s32[]{:S(2)}) async-start(), calls=%async_computation.6 | async-start | bytes 1351680 | tf_op jit(solution)/shard_map/all_gather | solution.py:95
  38.3 1.0 copy-start.2
  170.7 0.8 copy-start.9
  183.5 0.8 copy-start.9
  194.7 76.9 %all-gather.21.cloned.1.call-start = ((), (), s32[]{:S(2)}) async-start(), calls=%async_computation.5 | async-start | bytes 1310720 | tf_op jit(solution)/shard_map/all_gather | solution.py:77
  210.3 0.8 copy-start.17
  210.3 19.0 %copy-start.19 = (f32[2,1,128]{2,1,0:T(1,128)}, f32[2,1,128]{2,1,0:T(1,128)S(1)}, u32[]{:S(2)}) copy-start(f32[2,1,128]{2,1,0:T(1,128)S(1)} %get-tuple-element.151) | copy-start | bytes 3076
  210.3 64.6 %copy-start.10 = (f32[31,256]{1,0:T(8,128)S(1)}, f32[31,256]{1,0:T(8,128)}, u32[]{:S(2)}) copy-start(f32[31,256]{1,0:T(8,128)} %param.24) | copy-start | bytes 95236
  211.0 201.0 %all-gather.25.cloned.1.call-start = ((), (), s32[]{:S(2)}) async-start(), calls=%async_computation.7 | async-start | bytes 4595712 | tf_op jit(solution)/shard_map/all_gather | solution.py:95
  244.1 207.2 %all-gather.19.cloned.1.call-start = ((), (), s32[]{:S(2)}) async-start(), calls=%async_computation.4 | async-start | bytes 4456448 | tf_op jit(solution)/shard_map/all_gather | solution.py:77
  247.1 135.4 %copy-start.18 = (f32[2,1,128]{2,1,0:T(1,128)S(1)}, f32[2,1,128]{2,1,0:T(1,128)}, u32[]{:S(2)}) copy-start(f32[2,1,128]{2,1,0:T(1,128)} %copy-done.17) | copy-start | bytes 3076
  247.1 135.4 %copy-start.20 = (f32[2,1,128]{2,1,0:T(1,128)S(1)}, f32[2,1,128]{2,1,0:T(1,128)}, u32[]{:S(2)}) copy-start(f32[2,1,128]{2,1,0:T(1,128)} %copy-done.19) | copy-start | bytes 3076
  345.2 37.5 %collective-permute-start.1 = (bf16[15,256]{1,0:T(8,128)(2,1)S(1)}, bf16[15,256]{1,0:T(8,128)(2,1)S(1)}, u32[]{:S(2)}, u32[]{:S(2)}) collective-permute-start(bf16[15,256]{1,0:T(8,128)(2,1)S(1)} %get-tuple-element.463), channel_id=1, source_target_pairs={{8,0},{16,8},{24,16},{32,24},{40,32},{48,40},{56,48},{64,56},{72,6... | collective-permute-start | bytes 23048 | tf_op jit(solution)/shard_map/ppermute | solution.py:47
  346.5 36.2 %collective-permute-start = (bf16[15,256]{1,0:T(8,128)(2,1)S(1)}, bf16[15,256]{1,0:T(8,128)(2,1)S(1)}, u32[]{:S(2)}, u32[]{:S(2)}) collective-permute-start(bf16[15,256]{1,0:T(8,128)(2,1)S(1)} %get-tuple-element.462), channel_id=1, source_target_pairs={{0,8},{8,16},{16,24},{24,32},{32,40},{40,48},{48,56},{56,64},{64,7... | collective-permute-start | bytes 23048 | tf_op jit(solution)/shard_map/ppermute | solution.py:45
  382.7 21.9 %copy-start.24 = (f32[2,1]{0,1:T(1,128)S(1)}, f32[2,1]{0,1:T(1,128)}, u32[]{:S(2)}) copy-start(f32[2,1]{0,1:T(1,128)} %copy-done.23) | copy-start | bytes 28
  382.7 21.9 %copy-start.5 = (f32[2,1,128,256]{3,2,1,0:T(8,128)S(1)}, f32[2,1,128,256]{3,2,1,0:T(8,128)}, u32[]{:S(2)}) copy-start(f32[2,1,128,256]{3,2,1,0:T(8,128)} %get-tuple-element.163) | copy-start | bytes 786436
  382.7 26.5 %copy-start.13 = (f32[256]{0:T(256)S(1)}, f32[256]{0:T(256)}, u32[]{:S(2)}) copy-start(f32[256]{0:T(256)} %param.26) | copy-start | bytes 3076
  382.7 26.5 %copy-start.14 = (f32[256]{0:T(256)S(1)}, f32[256]{0:T(256)}, u32[]{:S(2)}) copy-start(f32[256]{0:T(256)} %param.25) | copy-start | bytes 3076
  383.9 61.7 %copy-start.12 = (f32[2,1,128]{2,1,0:T(1,128)S(1)}, f32[2,1,128]{2,1,0:T(1,128)}, u32[]{:S(2)}) copy-start(f32[2,1,128]{2,1,0:T(1,128)} %get-tuple-element.159) | copy-start | bytes 3076
  383.9 62.9 %copy-start.15 = (f32[2,1,128]{2,1,0:T(1,128)S(1)}, f32[2,1,128]{2,1,0:T(1,128)}, u32[]{:S(2)}) copy-start(f32[2,1,128]{2,1,0:T(1,128)} %get-tuple-element.164) | copy-start | bytes 3076
  383.9 62.9 %copy-start.16 = (f32[2,1,128]{2,1,0:T(1,128)S(1)}, f32[2,1,128]{2,1,0:T(1,128)}, u32[]{:S(2)}) copy-start(f32[2,1,128]{2,1,0:T(1,128)} %get-tuple-element.158) | copy-start | bytes 3076
  384.5 24.7 %all-to-all-start.1 = ((f32[8,1,512]{2,1,0:T(1,128)}), f32[8,1,512]{2,1,0:T(1,128)S(1)}, u32[]{:S(2)}, u32[]{:S(2)}) async-start(f32[8,1,512]{2,1,0:T(1,128)} %broadcast_in_dim.46), calls=%async_computation.1 | async-start | bytes 32768 | tf_op jit(solution)/shard_map/all_to_all | solution.py:23
  446.8 4.5 copy-start.4
  451.4 3.9 copy-start.3
  451.4 3.9 copy-start.6
  451.4 3.9 copy-start.21
  (3 other events, 1.9 us)
Sparse Core Ops, SparseCore 0:
  11.0 144.8 all-gather.16
  194.8 33.6 all-gather.22
  230.6 32.2 all-gather.20
  264.9 71.7 all-gather.24
  338.6 73.9 all-gather.18
where the time goes:
time: 484 us; the launch traced here: 481 us
  waiting for transfers between devices  148 us (31%)
  between operations  105 us (22%)
  blocking collectives  84 us (17%)
  other arithmetic  37.4 us (8%)
  starting transfers between devices  35.7 us (7%)
  local copies, waits for them, and re-layouts  34.8 us (7%)
  matrix products  30.9 us (6%)
  loops' own time  5.57 us (1%)
    all_gather x1, waiting for transfers between devices, sent_together(): filled = lax.all_gather(both, axis, axis=dim, tiled=True)  111 us
    unnamed x2, blocking collectives  35.7 us
    all_to_all x2, starting transfers between devices, sent_to_all(): return lax.all_to_all(copies, axis, split_axis=0, concat_axis=0, tiled=True)  30.3 us
    all_gather x2, blocking collectives, prefix_by_axis(): pieces = jax.tree.map(lambda part: lax.all_gather(part, axis), total)  30.2 us
    all_to_all x2, waiting for transfers between devices, sent_to_all(): return lax.all_to_all(copies, axis, split_axis=0, concat_axis=0, tiled=True)  19.3 us
    all_to_all x1, blocking collectives, sent_and_summed(): lax.all_to_all(split_up(array, dim, length), axis, 0, 0, tiled=True)  18.1 us
    all_gather x2, waiting for transfers between devices, gathered_once(): both, at, found = (lax.all_gather(jnp.concatenate(lines), axis), 0, {})  17.5 us
    unnamed x65, local copies, waits for them, and re-layouts  12 us
  transfers between devices with their start and end apart: 9, of which 4 were waited for; matrix products, arithmetic and copies ran while one was open for 12% of the time, Pallas kernels for 0%

commit v1 on v0

--- a/solution.py
+++ b/solution.py
@@ -1,16 +1,240 @@
+import functools
+
 import jax
 import jax.numpy as jnp
 from jax import lax
+from jax.experimental import pallas as pl
+from jax.experimental.pallas import tpu as pltpu
 from jax.sharding import Mesh
 from jax.sharding import PartitionSpec as P
+
+MESH = pl.DeviceIdType.MESH
+NZ, NY, NX = 16, 4, 4
+ROWS = 32
+TOKENS = 256
+D = 2048
+
+
+def ring(name, count):
+    me = lax.axis_index(name)
+
+    def at(step):
+        return lax.rem(me + (step % count), count)
+
+    return at
+
+
+def gather_project(
+    tok, wv, wg, wq, wk, wl, gain, gate_w, gate_b,
+    glu_o, q_o, k_o, v_o, gates_o,
+    wa, wb, rows_in, normed, own,
+    az_s, az_r, ay_s, ay_r, by_s, by_r, bz_s, bz_r, tx_s, tx_r, td_s, td_r,
+):
+    zat, yat, xat = ring("z", NZ), ring("y", NY), ring("x", NX)
+    core = lax.axis_index("c")
+    other = 1 - core
+
+    def up_z(ref_s, ref_r, src, dst, way):
+        return pltpu.make_async_remote_copy(src, dst, ref_s, ref_r, device_id={"z": zat(way)}, device_id_type=MESH)
+
+    def up_y(ref_s, ref_r, src, dst, way):
+        return pltpu.make_async_remote_copy(src, dst, ref_s, ref_r, device_id={"y": yat(way)}, device_id_type=MESH)
+
+    def up_x(ref_s, ref_r, src, dst, way):
+        return pltpu.make_async_remote_copy(src, dst, ref_s, ref_r, device_id={"x": xat(way)}, device_id_type=MESH)
+
+    def across(ref_s, ref_r, src, dst):
+        return pltpu.make_async_remote_copy(src, dst, ref_s, ref_r, device_id={"c": other}, device_id_type=MESH)
+
+    def row_at(dz, dy):
+        return pl.multiple_of((zat(dz) * NY + yat(dy)) * ROWS, ROWS)
+
+    sent = []
+
+    def go(copy):
+        copy.start()
+        sent.append(copy)
+        return copy
+
+    mine = row_at(0, 0)
+    a_own = [wv, wg, wq]
+    b_own = [wk, wl]
+    loads = []
+    for n, w in enumerate(a_own):
+        loads.append(pltpu.make_async_copy(w, wa.at[pl.ds(mine, ROWS), pl.ds(256 * n, 256)], own.at[n]))
+    for n, w in enumerate(b_own):
+        loads.append(pltpu.make_async_copy(w, wb.at[pl.ds(mine, ROWS), pl.ds(256 * n, 256)], own.at[3 + n]))
+    tp_own = xat(0) * 2 + core
+    loads.append(pltpu.make_async_copy(tok, rows_in.at[tp_own], own.at[5]))
+    for copy in loads:
+        copy.start()
+
+    barrier = pltpu.get_barrier_semaphore()
+    for dev in ({"z": zat(1)}, {"z": zat(-1)}, {"y": yat(1)}, {"y": yat(-1)}, {"x": xat(1)}, {"x": xat(-1)}, {"c": other}):
+        pl.semaphore_signal(barrier, inc=1, device_id=dev, device_id_type=MESH)
+    pl.semaphore_wait(barrier, 7)
+
+    def a_block(dz, dy, lo=0, size=ROWS):
+        return wa.at[pl.ds(pl.multiple_of(row_at(dz, dy) + lo, 16), size), :]
+
+    def b_block(dz, dy, lo=0, size=ROWS):
+        return wb.at[pl.ds(pl.multiple_of(row_at(dz, dy) + lo, 16), size), :]
+
+    def b_group(dz, lo=0, size=ROWS * NY):
+        return wb.at[pl.ds(pl.multiple_of(zat(dz) * (ROWS * NY) + lo, 64), size), :]
+
+    def send_az(way, s):
+        sign = 1 if way == 0 else -1
+        dz = -sign * (s - 1)
+        if s < 8:
+            block = a_block(dz, 0)
+        else:
+            block = a_block(dz, 0, 16 * way, 16)
+        return go(up_z(az_s.at[way, s - 1], az_r.at[way, s - 1], block, block, sign))
+
+    def send_bz(way, s):
+        sign = 1 if way == 0 else -1
+        dz = -sign * (s - 1)
+        if s < 8:
+            block = b_group(dz)
+        else:
+            block = b_group(dz, 64 * way, 64)
+        return go(up_z(bz_s.at[way, s - 1], bz_r.at[way, s - 1], block, block, sign))
+
+    def y_first(n, dz):
+        block = a_block(dz, 0)
+        return [go(up_y(ay_s.at[n, w], ay_r.at[n, w], block, block, 1 - 2 * w)) for w in range(2)]
+
+    def y_second(n, dz, first):
+        second = []
+        for w in range(2):
+            first[w].wait_recv()
+            sign = 1 - 2 * w
+            block = a_block(dz, -sign, 16 * w, 16)
+            second.append(go(up_y(ay_s.at[n, 2 + w], ay_r.at[n, 2 + w], block, block, sign)))
+        return second
+
+    for copy in loads[:3]:
+        copy.wait()
+    az = [send_az(0, 1), send_az(1, 1)]
+    for copy in loads[3:5]:
+        copy.wait()
+    by1 = []
+    for w in range(2):
+        block = b_block(0, 0)
+        by1.append(go(up_y(by_s.at[w], by_r.at[w], block, block, 1 - 2 * w)))
+    loads[5].wait()
+    tx1 = []
+    for w in range(2):
+        block = rows_in.at[tp_own]
+        tx1.append(go(up_x(tx_s.at[w], tx_r.at[w], block, block, 1 - 2 * w)))
+    td = [go(across(td_s.at[0], td_r.at[0], rows_in.at[tp_own], rows_in.at[tp_own]))]
+    ay_next = [(0, 0, y_first(0, 0))]
+
+    by2 = []
+    for w in range(2):
+        by1[w].wait_recv()
+        sign = 1 - 2 * w
+        block = b_block(0, -sign, 16 * w, 16)
+        by2.append(go(up_y(by_s.at[2 + w], by_r.at[2 + w], block, block, sign)))
+    tx2 = []
+    for w in range(2):
+        tx1[w].wait_recv()
+        sign = 1 - 2 * w
+        slot = xat(-sign) * 2 + core
+        half = rows_in.at[slot, pl.ds(128 * w, 128)]
+        tx2.append(go(up_x(tx_s.at[2 + w], tx_r.at[2 + w], half, half, sign)))
+        td.append(go(across(td_s.at[1 + w], td_r.at[1 + w], rows_in.at[slot], rows_in.at[slot])))
+    for copy in by2:
+        copy.wait_recv()
+    bz = [send_bz(0, 1), send_bz(1, 1)]
+
+    ay_last = []
+    for s in range(1, 9):
+        fresh = []
+        for w in range(2):
+            sign = 1 if w == 0 else -1
+            az[w].wait_recv()
+            if s < 8:
+                az[w] = send_az(w, s + 1)
+                n = s if w == 0 else 7 + s
+                fresh.append((n, -sign * s, y_first(n, -sign * s)))
+        if s == 8:
+            fresh.append((15, 8, y_first(15, 8)))
+        for w in range(2):
+            bz[w].wait_recv()
+            if s < 8:
+                bz[w] = send_bz(w, s + 1)
+        for n, dz, first in ay_next:
+            ay_last.extend(y_second(n, dz, first))
+        ay_next = fresh
+        if s == 1:
+            slot = xat(2) * 2 + core
+            for w in range(2):
+                tx2[w].wait_recv()
+                half = rows_in.at[slot, pl.ds(128 * w, 128)]
+                td.append(go(across(td_s.at[3 + w], td_r.at[3 + w], half, half)))
+        if s == 2:
+            for copy in td:
+                copy.wait_recv()
+            square = jnp.zeros((TOKENS, 256), jnp.float32)
+            for b in range(8):
+                wide = rows_in[b].astype(jnp.float32)
+                square = square + wide * wide
+            scale = lax.rsqrt(jnp.sum(square, axis=1, keepdims=True) / D + 1e-6)
+            for b in range(8):
+                cols = slice(256 * b, 256 * b + 256)
+                normed[:, cols] = (rows_in[b].astype(jnp.float32) * scale * gain[:, cols]).astype(jnp.bfloat16)
+            gates_o[...] = jnp.dot(normed[...], gate_w[...], preferred_element_type=jnp.float32) + gate_b[...]
+    for n, dz, first in ay_next:
+        ay_last.extend(y_second(n, dz, first))
+    k_o[...] = jnp.dot(normed[...], wb[:, 0:256], preferred_element_type=jnp.float32).astype(jnp.bfloat16)
+    v_o[...] = jnp.dot(normed[...], wb[:, 256:512], preferred_element_type=jnp.float32).astype(jnp.bfloat16)
+    for copy in ay_last:
+        copy.wait_recv()
+    value = jnp.dot(normed[...], wa[:, 0:256], preferred_element_type=jnp.float32)
+    gate = jnp.dot(normed[...], wa[:, 256:512], preferred_element_type=jnp.float32)
+    glu_o[...] = (value * jax.nn.sigmoid(gate)).astype(jnp.bfloat16)
+    q_o[...] = jnp.dot(normed[...], wa[:, 512:768], preferred_element_type=jnp.float32).astype(jnp.bfloat16)
+    for copy in sent:
+        copy.wait_send()
+
+
+def projected(tokens, weights, norm_gain, gate_weight, gate_bias):
+    vmem = pl.BlockSpec(memory_space=pltpu.VMEM)
+    hbm = pl.BlockSpec(memory_space=pl.ANY)
+    bf = jnp.bfloat16
+    dma = pltpu.SemaphoreType.DMA
+    return pl.pallas_call(
+        gather_project,
+        out_shape=[jax.ShapeDtypeStruct((TOKENS, 256), bf)] * 4 + [jax.ShapeDtypeStruct((TOKENS, 32), jnp.float32)],
+        in_specs=[hbm] * 6 + [vmem] * 3,
+        out_specs=[vmem] * 5,
+        scratch_shapes=[
+            pltpu.VMEM((D, 768), bf),
+            pltpu.VMEM((D, 512), bf),
+            pltpu.VMEM((8, TOKENS, 256), bf),
+            pltpu.VMEM((TOKENS, D), bf),
+            dma((6,)),
+            dma((2, 8)), dma((2, 8)),
+            dma((16, 4)), dma((16, 4)),
+            dma((4,)), dma((4,)),
+            dma((2, 8)), dma((2, 8)),
+            dma((4,)), dma((4,)),
+            dma((5,)), dma((5,)),
+        ],
+        compiler_params=pltpu.CompilerParams(collective_id=0, has_side_effects=True, vmem_limit_bytes=40 * 1024 * 1024),
+        name="gather_project",
+    )(tokens, *weights, norm_gain.reshape(1, D), gate_weight, gate_bias.reshape(1, 32))
 
 CONV = 2048
 MEMORY_HEADS = 8
 HEAD = 256
 KW = 31
 BLOCK = 128
-SP = ("sp_0", "sp_1")
-SP_TP = ("sp_0", "sp_1", "tp")
+SP = ("z", "y")
+SP_TP = ("z", "y", "x", "c")
+TP = ("x", "c")
 
 
 EPS = 1e-06
@@ -266,17 +490,13 @@
     out_conv,
     out_mem,
 ):
-    whole_rows = collect(tokens, "tp", 1)
-    wide = whole_rows.astype(jnp.float32)
-    normed = (
-        wide * lax.rsqrt(jnp.mean(wide * wide, axis=-1, keepdims=True) + EPS) * norm_gain
-    ).astype(jnp.bfloat16)
-    row_count = normed.shape[0]
+    glu, *projected_rows, gate_sums = projected(
+        tokens, (glu_value, glu_gate, query_weight, key_weight, value_weight), norm_gain, gate_weight, gate_bias
+    )
+    row_count = glu.shape[0]
     head_count = mem_gain.shape[0] // HEAD
-    first_head = lax.axis_index("tp") * head_count
-    gate_all = (
-        jnp.dot(normed, gate_weight, preferred_element_type=jnp.float32) + gate_bias
-    ).reshape(row_count, 4, MEMORY_HEADS)
+    first_head = lax.axis_index(TP) * head_count
+    gate_all = gate_sums.reshape(row_count, 4, MEMORY_HEADS)
     own_gates = lax.dynamic_slice_in_dim(gate_all, first_head, head_count, 2)
     own_extra = lax.dynamic_slice_in_dim(
         log_decay_extra.reshape(row_count, 2, MEMORY_HEADS), first_head, head_count, 2
@@ -326,12 +546,6 @@
             .astype(jnp.bfloat16)
         )
 
-    pieces = sent_together((glu_value, glu_gate, query_weight, key_weight, value_weight), SP, 0, 1)
-    sums = tuple(
-        (jnp.dot(normed, weight_rows, preferred_element_type=jnp.float32) for weight_rows in pieces)
-    )
-    glu = (sums[0] * jax.nn.sigmoid(sums[1])).astype(jnp.bfloat16)
-    projected = tuple((each_sum.astype(jnp.bfloat16) for each_sum in sums[2:]))
     reach = KW // 2
     padded = extended(glu, ((SP, 0),), reach).astype(jnp.float32)
     conv = jnp.zeros(glu.shape, jnp.float32)
@@ -339,42 +553,42 @@
         conv = conv + conv_taps[offset] * padded[offset : offset + row_count]
     chan_sums = jnp.sum(conv, axis=-1)
     chan_squares = jnp.sum(conv * conv, axis=-1)
-    chan_sums, chan_squares = together((chan_sums, chan_squares), "tp")
+    chan_sums, chan_squares = together((chan_sums, chan_squares), TP)
     chan_mean = chan_sums / CONV
     chan_var = chan_squares / CONV - chan_mean * chan_mean
     normal = (conv - chan_mean[:, None]) * lax.rsqrt(chan_var + EPS)[:, None] * ln_gain + ln_bias
     act = (normal * jax.nn.sigmoid(normal)).astype(jnp.bfloat16)
-    memory = memory_branch(*projected)
+    memory = memory_branch(*projected_rows)
     result = jnp.dot(act, out_conv, preferred_element_type=jnp.float32)
     mixed = sent_and_summed(
         (result + jnp.dot(memory, out_mem, preferred_element_type=jnp.float32)).astype(
             jnp.bfloat16
         ),
-        "tp",
+        TP,
         0,
     )
     return mixed.astype(jnp.bfloat16)
 
 
 def solution(mesh):
-    split = Mesh(mesh.devices.reshape(16, 4, mesh.shape["tp"]), ("sp_0", "sp_1", "tp"))
+    split = Mesh(mesh.devices.reshape(16, 4, 4, 2), ("z", "y", "x", "c"))
     placed = (
-        P(SP, "tp"),
+        P(SP, TP),
         P(),
-        P(SP, "tp"),
-        P(SP, "tp"),
-        P(None, "tp"),
-        P("tp"),
-        P("tp"),
-        P(SP, "tp"),
-        P(SP, "tp"),
-        P(SP, "tp"),
+        P(SP, TP),
+        P(SP, TP),
+        P(None, TP),
+        P(TP),
+        P(TP),
+        P(SP, TP),
+        P(SP, TP),
+        P(SP, TP),
         P(),
         P(),
         P(SP, None),
-        P("tp"),
-        P("tp", None),
-        P("tp", None),
+        P(TP),
+        P(TP, None),
+        P(TP, None),
     )
     return jax.shard_map(
         shards, mesh=split, in_specs=placed, out_specs=P(SP_TP, None), check_vma=False

time: 484 us -> 376 us (0.78)
  waiting for transfers between devices: 148 us -> 19.6 us
  Pallas kernels: 0 us -> 60.9 us
  matrix products: 30.9 us -> 16.6 us
  other arithmetic: 37.4 us -> 27.1 us
  starting transfers between devices: 35.7 us -> 25.8 us
    all_gather x1 -> x0, waiting for transfers between devices: 111 us -> none  [sent_together(): filled = lax.all_gather(both, axis, axis=dim, tiled=True)]
    pallas_call x0 -> x1, Pallas kernels: none -> 60.9 us  [projected(): pl.pallas_call(gather_project, out_shape=[jax.ShapeDtypeStruct((TOKENS, 2...]
    all_to_all x2 -> x1, waiting for transfers between devices: 19.3 us -> 3.03 us  [sent_to_all(): return lax.all_to_all(copies, axis, split_axis=0, concat_axis=0, tiled=True)]
    all_to_all x2 -> x1, starting transfers between devices: 30.3 us -> 20.4 us  [sent_to_all(): return lax.all_to_all(copies, axis, split_axis=0, concat_axis=0, tiled=True)]
    dot_general x6 -> x0, matrix products: 8.77 us -> none  [the longest x5 8.54 us: shards(): jnp.dot(normed, weight_rows, preferred_element_type=jnp.float32)]
    unnamed x65 -> x57, local copies, waits for them, and re-layouts: 12 us -> 13.8 us
  transfers between devices with their start and end apart: 9 -> 7, of which waited for: 4 -> 2; matrix products, arithmetic and copies ran while one was open for 12% -> 13% of each run, Pallas kernels for 0% -> 0%
where the time goes in v1:
time: 376 us; the launch traced here: 374 us
  between operations  104 us (28%)
  blocking collectives  82.9 us (22%)
  Pallas kernels  60.9 us (16%)
  local copies, waits for them, and re-layouts  31.4 us (8%)
  other arithmetic  27.1 us (7%)
  starting transfers between devices  25.8 us (7%)
  waiting for transfers between devices  19.6 us (5%)
  matrix products  16.6 us (4%)
  loops' own time  5.49 us (1%)
    pallas_call x1, Pallas kernels, projected(): pl.pallas_call(gather_project, out_shape=[jax.ShapeDtypeStruct((TOKENS, 2...  60.9 us
    unnamed x2, blocking collectives  35.7 us
    all_gather x2, blocking collectives, prefix_by_axis(): pieces = jax.tree.map(lambda part: lax.all_gather(part, axis), total)  29.2 us
    all_to_all x1, starting transfers between devices, sent_to_all(): return lax.all_to_all(copies, axis, split_axis=0, concat_axis=0, tiled=True)  20.4 us
    all_to_all x1, blocking collectives, sent_and_summed(): lax.all_to_all(split_up(array, dim, length), axis, 0, 0, tiled=True)  18 us
    all_gather x2, waiting for transfers between devices, gathered_once(): both, at, found = (lax.all_gather(jnp.concatenate(lines), axis), 0, {})  16.5 us
    unnamed x57, local copies, waits for them, and re-layouts  13.8 us
    dot_general x2, matrix products, finish(): jnp.einsum('htd,hde->hte', query_wide, in_mat, precision=PRECISE)  8.86 us
  transfers between devices with their start and end apart: 7, of which 2 were waited for; matrix products, arithmetic and copies ran while one was open for 13% of the time, Pallas kernels for 0%

profile of v1, /device:TPU:1, one launch (start us, length us, event | category | flops | bytes accessed | tf_op | source)
XLA Modules:
  0.0 373.6 jit_solution(10449929613399698157)
XLA Ops:
  13.7 60.9 %gather_project.1 = (bf16[256,256]{1,0:T(8,128)(2,1)S(1)}, bf16[256,256]{1,0:T(8,128)(2,1)S(1)}, bf16[256,256]{1,0:T(8,128)(2,1)S(1)}, bf16[256,256]{1,0:T(8,128)(2,1)S(1)}, f32[256,32]{1,0:T(8,128)S(1)}) custom-call(bf16[256,256]{1,0:T(8,128)(2,1)S(1)} %copy-done.1, bf16[32,256]{1,0:T(8,128)(2,1)S(1)} %copy-done.2, bf16[32,256]{1,0:T(8,128)(2,1)S(1)} %copy-done.3, ...), custom_call_target="tpu_custom_call" | custom-call | tf_op jit(solution)/shard_map/gather_project/pallas_call | solution.py:208
  77.1 11.3 %while.47 = (s32[]{:T(128)}, f32[1,256,256]{2,1,0:T(8,128)S(1)}, f32[1,256]{1,0:T(1,128)S(1)}, f32[1]{0:T(128)}, f32[2,1,128,256]{3,2,1,0:T(8,128)S(1)}, /*index...) while((s32[]{:T(128)}, f32[1,256,256]{2,1,0:T(8,128)S(1)}, ...), condition=%wide.region_17.18_spmd.clone, body=%wide.region_11.17_spmd.clone.sunk | while | flops 135383168 | bytes 1796895 | solution.py:419
  78.7 1.3 fusion.728
  84.3 1.3 fusion.728
  91.9 11.5 %while.46 = (s32[]{:T(128)}, f32[1,256,256]{2,1,0:T(8,128)S(1)}, f32[1,256]{1,0:T(1,128)S(1)}, f32[1]{0:T(128)}, f32[2,1,128,256]{3,2,1,0:T(8,128)S(1)}, /*index...) while((s32[]{:T(128)}, f32[1,256,256]{2,1,0:T(8,128)S(1)}, ...), condition=%wide.region_9.10_spmd.clone, body=%wide.region_3.9_spmd.clone.sunk | while | flops 135383168 | bytes 1796895 | solution.py:419
  93.6 1.3 fusion.711
  99.4 1.3 fusion.711
  104.2 16.5 %all-gather.20.cloned.1.call-done = f32[4,259,256]{2,1,0:T(8,128)} async-done(((f32[1,259,256]{2,1,0:T(8,128)}), f32[4,259,256]{2,1,0:T(8,128)}) %all-gather.20.cloned.1.call-update) | async-done | bytes 1060880 | tf_op jit(solution)/shard_map/all_gather | solution.py:319
  133.1 1.3 fusion.458
  134.4 1.3 fusion.666
  138.1 1.3 dynamic-slice
  140.1 2.1 fusion.552
  142.2 8.0 %all-reduce.9 = (f32[4]{0:T(128)S(1)}, f32[4]{0:T(128)S(1)}) all-reduce(f32[4]{0:T(128)S(1)} %dynamic-update-slice.2, f32[4]{0:T(128)S(1)} %fusion.552), channel_id=4, replica_groups=mesh['z'=16,'y'=4,'x'=4,'c'=2] {'y'}, use_global_device_ids=true, to_apply=%add.6 | all-reduce | flops 8 | bytes 64
  150.9 1.3 slice_add_fusion
  152.2 1.3 slice_maximum_fusion
  163.7 2.0 fusion.147
  165.8 1.3 collective-permute-start.1
  167.1 4.0 %collective-permute-start = (bf16[15,256]{1,0:T(8,128)(2,1)S(1)}, bf16[15,256]{1,0:T(8,128)(2,1)S(1)}, u32[]{:S(2)}, u32[]{:S(2)}) collective-permute-start(bf16[15,256]{1,0:T(8,128)(2,1)S(1)} %get-tuple-element.472), channel_id=1, source_target_pairs={{0,8},{8,16},{16,24},{24,32},{32,40},{40,48},{48,56},{56,64},{64,7... | collective-permute-start | bytes 23048 | tf_op jit(solution)/shard_map/ppermute | solution.py:269
  174.2 1.3 dynamic-slice.1
  175.5 1.3 dynamic-update-slice.3
  176.8 1.3 dynamic-update-slice.1
  178.1 27.7 %all-reduce.8 = (f32[16]{0:T(128)S(1)}, f32[16]{0:T(128)S(1)}) all-reduce(f32[16]{0:T(128)S(1)} %dynamic-update-slice.1, f32[16]{0:T(128)S(1)} %dynamic-update-slice.3), channel_id=3, replica_groups=mesh['z'=16,'y'=4,'x'=4,'c'=2] {'z'}, use_global_device_ids=true, to_apply=%add.5 | all-reduce | flops 32 | bytes 256
  240.5 7.8 %all-gather.8 = f32[4,1,256]{2,1,0:T(1,128)S(1)} all-gather(f32[1,1,256]{2,1,0:T(1,128)S(1)} %bitcast.722), channel_id=7, replica_groups=mesh['z'=16,'y'=4,'x'=4,'c'=2] {'y'}, dimensions={0}, use_global_device_ids=true | all-gather | bytes 5120 | tf_op jit(solution)/shard_map/all_gather | solution.py:301
  248.3 21.4 %all_gather.69 = f32[16,1,256]{2,1,0:T(1,128)S(1)} all-gather(f32[1,1,256]{2,1,0:T(1,128)S(1)} %get-tuple-element.451), channel_id=1, replica_groups=mesh['z'=16,'y'=4,'x'=4,'c'=2] {'z'}, dimensions={0}, use_global_device_ids=true | all-gather | bytes 17408 | tf_op jit(solution)/shard_map/all_gather | solution.py:301
  270.8 1.8 fusion.639
  273.2 20.4 %all-to-all-start = ((f32[8,1,512]{2,1,0:T(1,128)}), f32[8,1,512]{2,1,0:T(1,128)S(1)}, u32[]{:S(2)}, u32[]{:S(2)}) async-start(f32[8,1,512]{2,1,0:T(1,128)} %broadcast_in_dim.43), calls=%async_computation | async-start | bytes 32768 | tf_op jit(solution)/shard_map/all_to_all | solution.py:247
  295.3 3.0 all-to-all-done
  298.4 1.5 fusion.289
  335.6 4.9 %fusion.98 = f32[256,256]{0,1:T(8,128)} fusion(bf16[256,256]{1,0:T(8,128)(2,1)S(1)} %bitcast.712, f32[16,259,256]{2,1,0:T(8,128)} %all-gather.22.cloned.1.call-done, f32[256,256]{0,1:T(8,128)} %copy.124, f32[4,259,256]{2,1,0:T(8,128)} %all-gather.20.cloned.1.call-done, f32[256]{0:T(256)S(1)} %get-tuple-element.552, f32[]{:T(128)} %bitcast.275, ...), kind=kOutput, calls=%fused_computation.139 | convolution fusion | flops 207552512 | bytes 6723584 | tf_op jit(solution)/shard_map/htd,hde->hte/dot_general | solution.py:466
  340.6 3.1 reverse.15
  343.7 3.9 %multiply_reduce_fusion = (f32[256]{0:T(256)S(1)}, f32[256,256]{0,1:T(8,128)S(1)}) fusion(f32[256,256]{0,1:T(8,128)} %reverse.15, f32[256]{0:T(256)S(1)} %copy-done.16, bf16[256,256]{1,0:T(8,128)(2,1)S(1)} %bitcast.709, f32[16,1,256,256]{3,2,1,0:T(8,128)} %all-gather.16.cloned.1.call-done, f32[1,1,256,256]{3,2,1,0:T(8,128)} %fusion.147, ...), kind=kOutput, calls=%fused_computation.301 | convolution fusion | flops 207027968 | bytes 6196224 | tf_op jit(solution)/shard_map/htd,hde->hte/dot_general | solution.py:466
  348.3 18.0 %all_to_all.11 = bf16[8,32,2048]{2,1,0:T(8,128)(2,1)S(1)} all-to-all(bf16[8,32,2048]{2,1,0:T(8,128)(2,1)S(1)} %bitcast.715), channel_id=1, replica_groups=mesh['z'=16,'y'=4,'x'=4,'c'=2] {'x','c'}, dimensions={0} | all-to-all | bytes 2097152 | tf_op jit(solution)/shard_map/all_to_all | solution.py:358
  (187 shorter events, 40.5 us)
Async XLA Ops:
  6.5 291.8 %copy-start = (bf16[256,2048]{1,0:T(8,128)(2,1)S(1)}, bf16[256,2048]{1,0:T(8,128)(2,1)}, u32[]{:S(2)}) copy-start(bf16[256,2048]{1,0:T(8,128)(2,1)} %param.34) | copy-start | bytes 3145732
  6.5 114.2 %all-gather.20.cloned.1.call-start = ((), (), s32[]{:S(2)}) async-start(), calls=%async_computation.4 | async-start | bytes 1351680 | tf_op jit(solution)/shard_map/all_gather | solution.py:319
  7.8 0.9 copy-start.1
  8.8 0.7 copy-start.2
  9.5 0.7 copy-start.3
  10.2 0.7 copy-start.4
  10.9 0.7 copy-start.5
  11.6 0.7 copy-start.6
  12.3 0.7 copy-start.7
  13.0 0.7 copy-start.8
  91.8 71.9 %all-gather.18.cloned.1.call-start = ((), (), s32[]{:S(2)}) async-start(), calls=%async_computation.3 | async-start | bytes 1310720 | tf_op jit(solution)/shard_map/all_gather | solution.py:301
  103.4 0.7 copy-start.9
  104.2 196.4 %all-gather.22.cloned.1.call-start = ((), (), s32[]{:S(2)}) async-start(), calls=%async_computation.5 | async-start | bytes 4595712 | tf_op jit(solution)/shard_map/all_gather | solution.py:319
  134.4 135.4 %copy-start.11 = (f32[31,256]{1,0:T(8,128)S(1)}, f32[31,256]{1,0:T(8,128)}, u32[]{:S(2)}) copy-start(f32[31,256]{1,0:T(8,128)} %param.24) | copy-start | bytes 95236
  136.4 207.2 %all-gather.16.cloned.1.call-start = ((), (), s32[]{:S(2)}) async-start(), calls=%async_computation.2 | async-start | bytes 4456448 | tf_op jit(solution)/shard_map/all_gather | solution.py:301
  165.8 105.0 %collective-permute-start.1 = (bf16[15,256]{1,0:T(8,128)(2,1)S(1)}, bf16[15,256]{1,0:T(8,128)(2,1)S(1)}, u32[]{:S(2)}, u32[]{:S(2)}) collective-permute-start(bf16[15,256]{1,0:T(8,128)(2,1)S(1)} %get-tuple-element.473), channel_id=1, source_target_pairs={{8,0},{16,8},{24,16},{32,24},{40,32},{48,40},{56,48},{64,56},{72,6... | collective-permute-start | bytes 23048 | tf_op jit(solution)/shard_map/ppermute | solution.py:271
  167.1 103.7 %collective-permute-start = (bf16[15,256]{1,0:T(8,128)(2,1)S(1)}, bf16[15,256]{1,0:T(8,128)(2,1)S(1)}, u32[]{:S(2)}, u32[]{:S(2)}) collective-permute-start(bf16[15,256]{1,0:T(8,128)(2,1)S(1)} %get-tuple-element.472), channel_id=1, source_target_pairs={{0,8},{8,16},{16,24},{24,32},{32,40},{40,48},{48,56},{56,64},{64,7... | collective-permute-start | bytes 23048 | tf_op jit(solution)/shard_map/ppermute | solution.py:269
  270.8 27.6 %copy-start.12 = (f32[256]{0:T(256)S(1)}, f32[256]{0:T(256)}, u32[]{:S(2)}) copy-start(f32[256]{0:T(256)} %param.26) | copy-start | bytes 3076
  270.8 27.6 %copy-start.13 = (f32[256]{0:T(256)S(1)}, f32[256]{0:T(256)}, u32[]{:S(2)}) copy-start(f32[256]{0:T(256)} %param.25) | copy-start | bytes 3076
  273.2 25.1 %all-to-all-start = ((f32[8,1,512]{2,1,0:T(1,128)}), f32[8,1,512]{2,1,0:T(1,128)S(1)}, u32[]{:S(2)}, u32[]{:S(2)}) async-start(f32[8,1,512]{2,1,0:T(1,128)} %broadcast_in_dim.43), calls=%async_computation | async-start | bytes 32768 | tf_op jit(solution)/shard_map/all_to_all | solution.py:247
  295.3 39.2 %copy-start.14 = (f32[1,1,256]{2,1,0:T(1,128)S(1)}, f32[1,1,256]{2,1,0:T(1,128)}, u32[]{:S(2)}) copy-start(f32[1,1,256]{2,1,0:T(1,128)} %get-tuple-element.454) | copy-start | bytes 3076
  335.6 8.1 %copy-start.15 = (f32[256]{0:T(256)S(1)}, f32[256]{0:T(256)}, u32[]{:S(2)}) copy-start(f32[256]{0:T(256)} %get-tuple-element.548) | copy-start | bytes 3076
  335.6 8.1 %copy-start.16 = (f32[256]{0:T(256)S(1)}, f32[256]{0:T(256)}, u32[]{:S(2)}) copy-start(f32[256]{0:T(256)} %get-tuple-element.549) | copy-start | bytes 3076
  335.6 8.1 %copy-start.17 = (f32[256]{0:T(256)S(1)}, f32[256]{0:T(256)}, u32[]{:S(2)}) copy-start(f32[256]{0:T(256)} %get-tuple-element.550) | copy-start | bytes 3076
  343.7 4.0 %copy-start.10 = (bf16[256,2048]{1,0:T(8,128)(2,1)S(1)}, bf16[256,2048]{1,0:T(8,128)(2,1)}, u32[]{:S(2)}) copy-start(bf16[256,2048]{1,0:T(8,128)(2,1)} %param.35) | copy-start | bytes 3145732
  343.7 4.0 %copy-start.18 = (f32[256]{0:T(256)S(1)}, f32[256]{0:T(256)}, u32[]{:S(2)}) copy-start(f32[256]{0:T(256)} %param.33) | copy-start | bytes 3076
Sparse Core Ops, SparseCore 0:
  91.9 28.7 all-gather.19
  122.8 32.3 all-gather.17
  157.2 72.0 all-gather.21
  231.3 73.5 all-gather.15

commit v2 on v1

v2 whole, which is shorter than its diff:
```python
import functools

import jax
import jax.numpy as jnp
from jax import lax
from jax.experimental import pallas as pl
from jax.experimental.pallas import tpu as pltpu
from jax.sharding import Mesh
from jax.sharding import PartitionSpec as P

MESH = pl.DeviceIdType.MESH
NZ, NY, NX = 16, 4, 4
ROWS = 32
TOKENS = 256
D = 2048


def ring(name, count):
    me = lax.axis_index(name)

    def at(step):
        return lax.rem(me + (step % count), count)

    return at


def gather_project(
    tok, wv, wg, wq, wk, wl, gain, gate_w, gate_b,
    glu_o, q_o, k_o, v_o, gates_o,
    wa, wb, rows_in, normed, own,
    az_s, az_r, ay_s, ay_r, by_s, by_r, bz_s, bz_r, tx_s, tx_r, td_s, td_r,
):
    zat, yat, xat = ring("z", NZ), ring("y", NY), ring("x", NX)
    core = lax.axis_index("c")
    other = 1 - core

    def up_z(ref_s, ref_r, src, dst, way):
        return pltpu.make_async_remote_copy(src, dst, ref_s, ref_r, device_id={"z": zat(way)}, device_id_type=MESH)

    def up_y(ref_s, ref_r, src, dst, way):
        return pltpu.make_async_remote_copy(src, dst, ref_s, ref_r, device_id={"y": yat(way)}, device_id_type=MESH)

    def up_x(ref_s, ref_r, src, dst, way):
        return pltpu.make_async_remote_copy(src, dst, ref_s, ref_r, device_id={"x": xat(way)}, device_id_type=MESH)

    def across(ref_s, ref_r, src, dst):
        return pltpu.make_async_remote_copy(src, dst, ref_s, ref_r, device_id={"c": other}, device_id_type=MESH)

    def row_at(dz, dy):
        return pl.multiple_of((zat(dz) * NY + yat(dy)) * ROWS, ROWS)

    sent = []

    def go(copy):
        copy.start()
        sent.append(copy)
        return copy

    mine = row_at(0, 0)
    a_own = [wv, wg, wq]
    b_own = [wk, wl]
    loads = []
    for n, w in enumerate(a_own):
        loads.append(pltpu.make_async_copy(w, wa.at[pl.ds(mine, ROWS), pl.ds(256 * n, 256)], own.at[n]))
    for n, w in enumerate(b_own):
        loads.append(pltpu.make_async_copy(w, wb.at[pl.ds(mine, ROWS), pl.ds(256 * n, 256)], own.at[3 + n]))
    tp_own = xat(0) * 2 + core
    loads.append(pltpu.make_async_copy(tok, rows_in.at[tp_own], own.at[5]))
    for copy in loads:
        copy.start()

    barrier = pltpu.get_barrier_semaphore()
    for dev in ({"z": zat(1)}, {"z": zat(-1)}, {"y": yat(1)}, {"y": yat(-1)}, {"x": xat(1)}, {"x": xat(-1)}, {"c": other}):
        pl.semaphore_signal(barrier, inc=1, device_id=dev, device_id_type=MESH)
    pl.semaphore_wait(barrier, 7)

    def a_block(dz, dy, lo=0, size=ROWS):
        return wa.at[pl.ds(pl.multiple_of(row_at(dz, dy) + lo, 16), size), :]

    def b_block(dz, dy, lo=0, size=ROWS):
        return wb.at[pl.ds(pl.multiple_of(row_at(dz, dy) + lo, 16), size), :]

    def b_group(dz, lo=0, size=ROWS * NY):
        return wb.at[pl.ds(pl.multiple_of(zat(dz) * (ROWS * NY) + lo, 64), size), :]

    def send_az(way, s):
        sign = 1 if way == 0 else -1
        dz = -sign * (s - 1)
        if s < 8:
            block = a_block(dz, 0)
        else:
            block = a_block(dz, 0, 16 * way, 16)
        return go(up_z(az_s.at[way, s - 1], az_r.at[way, s - 1], block, block, sign))

    def send_bz(way, s):
        sign = 1 if way == 0 else -1
        dz = -sign * (s - 1)
        if s < 8:
            block = b_group(dz)
        else:
            block = b_group(dz, 64 * way, 64)
        return go(up_z(bz_s.at[way, s - 1], bz_r.at[way, s - 1], block, block, sign))

    def y_first(n, dz):
        block = a_block(dz, 0)
        return [go(up_y(ay_s.at[n, w], ay_r.at[n, w], block, block, 1 - 2 * w)) for w in range(2)]

    def y_second(n, dz, first):
        second = []
        for w in range(2):
            first[w].wait_recv()
            sign = 1 - 2 * w
            block = a_block(dz, -sign, 16 * w, 16)
            second.append(go(up_y(ay_s.at[n, 2 + w], ay_r.at[n, 2 + w], block, block, sign)))
        return second

    for copy in loads[:3]:
        copy.wait()
    az = [send_az(0, 1), send_az(1, 1)]
    for copy in loads[3:5]:
        copy.wait()
    by1 = []
    for w in range(2):
        block = b_block(0, 0)
        by1.append(go(up_y(by_s.at[w], by_r.at[w], block, block, 1 - 2 * w)))
    loads[5].wait()
    tx1 = []
    for w in range(2):
        block = rows_in.at[tp_own]
        tx1.append(go(up_x(tx_s.at[w], tx_r.at[w], block, block, 1 - 2 * w)))
    td = [go(across(td_s.at[0], td_r.at[0], rows_in.at[tp_own], rows_in.at[tp_own]))]
    ay_next = [(0, 0, y_first(0, 0))]

    by2 = []
    for w in range(2):
        by1[w].wait_recv()
        sign = 1 - 2 * w
        block = b_block(0, -sign, 16 * w, 16)
        by2.append(go(up_y(by_s.at[2 + w], by_r.at[2 + w], block, block, sign)))
    tx2 = []
    for w in range(2):
        tx1[w].wait_recv()
        sign = 1 - 2 * w
        slot = xat(-sign) * 2 + core
        half = rows_in.at[slot, pl.ds(128 * w, 128)]
        tx2.append(go(up_x(tx_s.at[2 + w], tx_r.at[2 + w], half, half, sign)))
        td.append(go(across(td_s.at[1 + w], td_r.at[1 + w], rows_in.at[slot], rows_in.at[slot])))
    for copy in by2:
        copy.wait_recv()
    bz = [send_bz(0, 1), send_bz(1, 1)]

    ay_last = []
    for s in range(1, 9):
        fresh = []
        for w in range(2):
            sign = 1 if w == 0 else -1
            az[w].wait_recv()
            if s < 8:
                az[w] = send_az(w, s + 1)
                n = s if w == 0 else 7 + s
                fresh.append((n, -sign * s, y_first(n, -sign * s)))
        if s == 8:
            fresh.append((15, 8, y_first(15, 8)))
        for w in range(2):
            bz[w].wait_recv()
            if s < 8:
                bz[w] = send_bz(w, s + 1)
        for n, dz, first in ay_next:
            ay_last.extend(y_second(n, dz, first))
        ay_next = fresh
        if s == 1:
            slot = xat(2) * 2 + core
            for w in range(2):
                tx2[w].wait_recv()
                half = rows_in.at[slot, pl.ds(128 * w, 128)]
                td.append(go(across(td_s.at[3 + w], td_r.at[3 + w], half, half)))
        if s == 2:
            for copy in td:
                copy.wait_recv()
            square = jnp.zeros((TOKENS, 256), jnp.float32)
            for b in range(8):
                wide = rows_in[b].astype(jnp.float32)
                square = square + wide * wide
            scale = lax.rsqrt(jnp.sum(square, axis=1, keepdims=True) / D + 1e-6)
            for b in range(8):
                cols = slice(256 * b, 256 * b + 256)
                normed[:, cols] = (rows_in[b].astype(jnp.float32) * scale * gain[:, cols]).astype(jnp.bfloat16)
            gates_o[...] = jnp.dot(normed[...], gate_w[...], preferred_element_type=jnp.float32) + gate_b[...]
    for n, dz, first in ay_next:
        ay_last.extend(y_second(n, dz, first))
    k_o[...] = jnp.dot(normed[...], wb[:, 0:256], preferred_element_type=jnp.float32).astype(jnp.bfloat16)
    v_o[...] = jnp.dot(normed[...], wb[:, 256:512], preferred_element_type=jnp.float32).astype(jnp.bfloat16)
    for copy in ay_last:
        copy.wait_recv()
    value = jnp.dot(normed[...], wa[:, 0:256], preferred_element_type=jnp.float32)
    gate = jnp.dot(normed[...], wa[:, 256:512], preferred_element_type=jnp.float32)
    glu_o[...] = (value * jax.nn.sigmoid(gate)).astype(jnp.bfloat16)
    q_o[...] = jnp.dot(normed[...], wa[:, 512:768], preferred_element_type=jnp.float32).astype(jnp.bfloat16)
    for copy in sent:
        copy.wait_send()


def projected(tokens, weights, norm_gain, gate_weight, gate_bias):
    vmem = pl.BlockSpec(memory_space=pltpu.VMEM)
    hbm = pl.BlockSpec(memory_space=pltpu.HBM)
    bf = jnp.bfloat16
    dma = pltpu.SemaphoreType.DMA
    return pl.pallas_call(
        gather_project,
        out_shape=[jax.ShapeDtypeStruct((TOKENS, 256), bf)] * 4 + [jax.ShapeDtypeStruct((TOKENS, 32), jnp.float32)],
        in_specs=[hbm] * 6 + [vmem] * 3,
        out_specs=[vmem] * 5,
        scratch_shapes=[
            pltpu.VMEM((D, 768), bf),
            pltpu.VMEM((D, 512), bf),
            pltpu.VMEM((8, TOKENS, 256), bf),
            pltpu.VMEM((TOKENS, D), bf),
            dma((6,)),
            dma((2, 8)), dma((2, 8)),
            dma((16, 4)), dma((16, 4)),
            dma((4,)), dma((4,)),
            dma((2, 8)), dma((2, 8)),
            dma((4,)), dma((4,)),
            dma((5,)), dma((5,)),
        ],
        compiler_params=pltpu.CompilerParams(collective_id=0, has_side_effects=True, vmem_limit_bytes=40 * 1024 * 1024),
        name="gather_project",
    )(tokens, *weights, norm_gain.reshape(1, D), gate_weight, gate_bias.reshape(1, 32))
NEG = -1e30
EPS = 1e-06
F32 = jnp.float32
BF16 = jnp.bfloat16


def joined(state, level, new_state, new_level, decay):
    top = jnp.maximum(level + decay, new_level)
    early = jnp.exp(level + decay - top)
    late = jnp.exp(new_level - top)
    parts = []
    for old, new in zip(state, new_state):
        if old.ndim == 3:
            parts.append(early[None] * old + late[None] * new)
        else:
            parts.append(early * old + late * new)
    return tuple(parts), top


def log_sigmoid(x):
    return -(jnp.maximum(-x, 0.0) + jnp.log1p(jnp.exp(-jnp.abs(x))))


def mix(
    glu, q, k, v, gates, extra, taps, ln_gain, ln_bias, mem_gain, out_conv, out_mem,
    out,
    wc, wm, st, sm, ry, rsm, tz, gsm, rz, rgs, iz, ri, inc, rin,
    halo, ext, cv, stat, rstat, act, mem, num_f, num_b, psend, pown, precv, xsend, xrecv,
    wsem, h_s, h_r, y_s, y_r, ym_s, ym_r, z_s, z_r, zm_s, zm_r, zb_s, zb_r, yb_s, yb_r, t_s, t_r, d_s, d_r, o_s, o_r,
):
    zat, yat, xat = ring("z", NZ), ring("y", NY), ring("x", NX)
    z, y, x, core = lax.axis_index("z"), lax.axis_index("y"), lax.axis_index("x"), lax.axis_index("c")
    other = 1 - core
    head = x * 2 + core

    def remote(src, dst, ss, rs, dev):
        return pltpu.make_async_remote_copy(src, dst, ss, rs, device_id=dev, device_id_type=MESH)

    sent = []

    def go(copy):
        copy.start()
        sent.append(copy)
        return copy

    wide = [pltpu.make_async_copy(out_conv, wc, wsem.at[0]), pltpu.make_async_copy(out_mem, wm, wsem.at[1])]
    for copy in wide:
        copy.start()

    after = {"z": zat(lax.convert_element_type(y == NY - 1, jnp.int32)), "y": yat(1)}
    before = {"z": lax.rem(z + NZ - lax.convert_element_type(y == 0, jnp.int32), NZ), "y": yat(-1)}
    peers = [after, before]
    peers += [{"y": yat(dy)} for dy in range(1, NY)]
    peers += [{"z": zat(dz)} for dz in range(1, NZ)]
    peers += [{"x": xat(dx), "c": cc} for dx in range(1, NX) for cc in (core, other)] + [{"c": other}]
    barrier = pltpu.get_barrier_semaphore()
    for dev in peers:
        pl.semaphore_signal(barrier, inc=1, device_id=dev, device_id_type=MESH)

    lane = lax.broadcasted_iota(jnp.int32, (TOKENS, 32), 1)
    lane16 = lax.broadcasted_iota(jnp.int32, (TOKENS, 16), 1)
    t_at = lax.broadcasted_iota(jnp.int32, (TOKENS, TOKENS), 0)
    s_at = lax.broadcasted_iota(jnp.int32, (TOKENS, TOKENS), 1)

    def column(n):
        return jnp.sum(jnp.where(lane == 8 * n + head, gates[...], 0.0), axis=1, keepdims=True)

    def extra_column(n):
        return jnp.sum(jnp.where(lane16 == 8 * n + head, extra[...], 0.0), axis=1, keepdims=True)

    def as_row(col):
        return jnp.sum(jnp.where(t_at == s_at, col, 0.0), axis=0, keepdims=True)

    def as_column(row):
        return jnp.sum(jnp.where(t_at == s_at, row, 0.0), axis=1, keepdims=True)

    in_f, in_b = column(0), column(2)
    lf_f = log_sigmoid(column(1)) + extra_column(0)
    lf_b = log_sigmoid(column(3)) + extra_column(1)
    sum_f_row = jnp.sum(jnp.where(t_at <= s_at, lf_f, 0.0), axis=0, keepdims=True)
    sum_b_row = jnp.sum(jnp.where(t_at >= s_at, lf_b, 0.0), axis=0, keepdims=True)
    sum_f, sum_b = as_column(sum_f_row), as_column(sum_b_row)
    total_f = jnp.sum(lf_f, axis=0, keepdims=True)
    total_b = jnp.sum(lf_b, axis=0, keepdims=True)

    keys = k[...].astype(F32)

    def summary(total, sums, gate):
        to_end = total - sums + gate
        level = jnp.max(to_end, axis=0, keepdims=True)
        weighted = keys * (jnp.exp(to_end - level) * 0.0625)
        state = lax.dot_general(weighted.astype(BF16), v[...], (((0,), (0,)), ((), ())), preferred_element_type=F32)
        return state, jnp.sum(weighted, axis=0, keepdims=True), level

    state_f, vec_f, level_f = summary(total_f, sum_f, in_f)
    state_b, vec_b, level_b = summary(total_b, sum_b, in_b)
    for h in range(2):
        cols = slice(128 * h, 128 * h + 128)
        both = jnp.concatenate([state_f[:, cols].reshape(32, 8, 128), state_b[:, cols].reshape(32, 8, 128)], axis=1)
        st[32 * h : 32 * h + 32] = both.astype(BF16)
    for n, row in enumerate((vec_f[:, :128], vec_f[:, 128:], vec_b[:, :128], vec_b[:, 128:])):
        sm[n : n + 1, :] = row
    for n, one in enumerate((total_f, level_f, total_b, level_b)):
        sm[4 + n : 5 + n, :] = jnp.broadcast_to(one, (1, 128))
    ry[y] = st[pl.ds(y * 16, 16)]
    rsm[y] = sm[...]

    pl.semaphore_wait(barrier, len(peers))
    halos = [
        go(remote(glu.at[pl.ds(240, 16), :], halo.at[0], h_s.at[0], h_r.at[0], after)),
        go(remote(glu.at[pl.ds(0, 16), :], halo.at[1], h_s.at[1], h_r.at[1], before)),
    ]
    y_in = []
    for dy in range(1, NY):
        to = yat(dy)
        y_in.append(go(remote(sm, rsm.at[y], ym_s.at[dy], ym_r.at[dy], {"y": to})))
        y_in.append(go(remote(st.at[pl.ds(to * 16, 16)], ry.at[y], y_s.at[dy], y_r.at[dy], {"y": to})))

    scores = lax.dot_general(q[...], k[...], (((1,), (1,)), ((), ())), preferred_element_type=F32) * 0.0625

    def inside(mask, sums, sum_row, gate, numerator):
        log_weight = jnp.where(mask, sums - sum_row + as_row(gate), NEG)
        top = jnp.max(log_weight, axis=1, keepdims=True)
        weights = scores * jnp.exp(log_weight - top)
        numerator[...] = jnp.dot(weights.astype(BF16), v[...], preferred_element_type=F32)
        return jnp.sum(weights, axis=1, keepdims=True), top

    den_f, top_f = inside(s_at <= t_at, sum_f, sum_f_row, in_f, num_f)
    den_b, top_b = inside(s_at >= t_at, sum_b, sum_b_row, in_b, num_b)

    for copy in y_in:
        copy.wait_recv()

    def y_pieces(n, d):
        return ry[n].astype(F32)[:, 8 * d : 8 * d + 8, :], rsm[n, 2 * d : 2 * d + 2, :]

    def y_scalars(n, d):
        return rsm[n, 5 + 2 * d : 6 + 2 * d, :], rsm[n, 4 + 2 * d : 5 + 2 * d, :]

    def y_walk(d, start, level):
        state = start
        found = []
        for n in range(NY) if d == 0 else reversed(range(NY)):
            found.append((n, state, level))
            state, level = joined(state, level, y_pieces(n, d), *y_scalars(n, d))
        return found, state, level

    low = jnp.full((1, 128), NEG, F32)
    zero = (jnp.zeros((16, 8, 128), F32), jnp.zeros((2, 128), F32))
    groups = []
    for d in range(2):
        _, group, level = y_walk(d, zero, low)
        groups.append(group)
        gsm[2 * d : 2 * d + 2, :] = group[1]
        decay = low * 0.0
        for n in range(NY):
            decay = decay + y_scalars(n, d)[1]
        gsm[4 + 2 * d : 5 + 2 * d, :] = decay
        gsm[5 + 2 * d : 6 + 2 * d, :] = level
    tz[...] = jnp.concatenate([groups[0][0], groups[1][0]], axis=1).astype(BF16)
    rz[z] = tz[z]
    rgs[z] = gsm[...]
    z_in = []
    for dz in range(1, NZ):
        to = zat(dz)
        z_in.append(go(remote(tz.at[to], rz.at[z], z_s.at[dz], z_r.at[dz], {"z": to})))
        z_in.append(go(remote(gsm, rgs.at[z], zm_s.at[dz], zm_r.at[dz], {"z": to})))

    for copy in halos:
        copy.wait_recv()
    place = z * NY + y
    for h in range(2):
        cols = slice(128 * h, 128 * h + 128)
        ext[h, 0:16, :] = jnp.where(place == 0, 0.0, halo[0][:, cols].astype(F32))
        ext[h, 16:272, :] = glu[:, cols].astype(F32)
        ext[h, 272:288, :] = jnp.where(place == NZ * NY - 1, 0.0, halo[1][:, cols].astype(F32))
    for h in range(2):
        cols = slice(128 * h, 128 * h + 128)

        def rows_of(n, carry):
            first = n * 64
            total = jnp.zeros((64, 128), F32)
            for j in range(31):
                total = total + taps[j : j + 1, cols] * ext[h, pl.ds(first + (j + 1), 64), :]
            cv[pl.ds(pl.multiple_of(first, 64), 64), cols] = total
            return carry

        lax.fori_loop(0, 4, rows_of, 0)
    conv = cv[...]
    stat[0:1, :] = as_row(jnp.sum(conv, axis=1, keepdims=True))
    stat[1:2, :] = as_row(jnp.sum(conv * conv, axis=1, keepdims=True))
    stat[2:8, :] = jnp.zeros((6, TOKENS), F32)
    t_in = []
    tp_peers = [(dx, cc) for dx in range(NX) for cc in range(2) if dx or cc]
    for n, (dx, cc) in enumerate(tp_peers):
        dev = {"x": xat(dx), "c": core if cc == 0 else other}
        t_in.append(go(remote(stat, rstat.at[n], t_s.at[n], t_r.at[n], dev)))

    for copy in z_in:
        copy.wait_recv()
    came, came_level = [], []
    entering = []
    for d in range(2):
        state = (jnp.zeros((8, 128), F32), jnp.zeros((2, 128), F32))
        level = low
        kept, kept_level = jnp.zeros((2, 128), F32), low
        lines = [None] * NZ
        for n in range(NZ) if d == 0 else reversed(range(NZ)):
            lines[n] = state[0]
            kept = jnp.where(z == n, state[1], kept)
            kept_level = jnp.where(z == n, level, kept_level)
            piece = (rz[n].astype(F32)[8 * d : 8 * d + 8, :], rgs[n, 2 * d : 2 * d + 2, :])
            state, level = joined(state, level, piece, rgs[n, 5 + 2 * d : 6 + 2 * d, :], rgs[n, 4 + 2 * d : 5 + 2 * d, :])
        entering.append(lines)
        came.append(kept)
        came_level.append(kept_level)
    for n in range(NZ):
        iz[n] = jnp.concatenate([entering[0][n], entering[1][n]], axis=0).astype(BF16)
    ri[z] = iz[z]
    zb_in = []
    for dz in range(1, NZ):
        to = zat(dz)
        zb_in.append(go(remote(iz.at[to], ri.at[z], zb_s.at[dz], zb_r.at[dz], {"z": to})))

    sums = stat[...]
    for n, copy in enumerate(t_in):
        copy.wait_recv()
        sums = sums + rstat[n]
    mean = as_column(sums[0:1, :]) / CONV
    var = as_column(sums[1:2, :]) / CONV - mean * mean
    normal = (cv[...] - mean) * lax.rsqrt(var + EPS) * ln_gain[...] + ln_bias[...]
    act[...] = (normal * jax.nn.sigmoid(normal)).astype(BF16).reshape(8, 32, 256)
    for copy in wide:
        copy.wait()

    for copy in zb_in:
        copy.wait_recv()
    back = [None] * 2
    mine = []
    for d in range(2):
        start = (ri[...].astype(F32)[:, 8 * d : 8 * d + 8, :], came[d])
        found, _, _ = y_walk(d, start, came_level[d])
        kept, kept_level = jnp.zeros((2, 128), F32), low
        back[d] = [None] * NY
        for n, state, level in found:
            back[d][n] = state[0]
            kept = jnp.where(y == n, state[1], kept)
            kept_level = jnp.where(y == n, level, kept_level)
        mine.append((kept, kept_level))
    for n in range(NY):
        inc[n] = jnp.concatenate([back[0][n], back[1][n]], axis=1).astype(BF16)
    rin[y] = inc[y]
    yb_in = []
    for dy in range(1, NY):
        to = yat(dy)
        yb_in.append(go(remote(inc.at[to], rin.at[y], yb_s.at[dy], yb_r.at[dy], {"y": to})))
    for copy in yb_in:
        copy.wait_recv()

    def finished(d, numerator, den, top, sums):
        vec, level = mine[d]
        vec = jnp.concatenate([vec[0:1, :], vec[1:2, :]], axis=1)
        state = rin[...].reshape(64, 16, 128).astype(F32)[:, 8 * d : 8 * d + 8, :]
        left = state[:32].reshape(256, 128).astype(BF16)
        right = state[32:].reshape(256, 128).astype(BF16)
        carried = sums + level[:, 0:1]
        high = jnp.maximum(top, carried)
        near = jnp.exp(top - high)
        far = jnp.exp(carried - high)
        read = jnp.concatenate(
            [jnp.dot(q[...], left, preferred_element_type=F32), jnp.dot(q[...], right, preferred_element_type=F32)], axis=1
        )
        upper = near * numerator[...] + far * read
        lower = near * den + far * jnp.sum(q[...].astype(F32) * vec, axis=1, keepdims=True)
        return upper / jnp.maximum(jnp.abs(lower), jnp.exp(-high))

    summed = finished(0, num_f, den_f, top_f, sum_f) + finished(1, num_b, den_b, top_b, sum_b)
    scale = lax.rsqrt(jnp.mean(summed * summed, axis=1, keepdims=True) + EPS)
    mem[...] = (summed * scale * mem_gain[...]).astype(BF16).reshape(8, 32, 256)

    def part(c, dx):
        slot = xat(dx) * 2 + c
        return jnp.dot(act[slot], wc[...], preferred_element_type=F32) + jnp.dot(mem[slot], wm[...], preferred_element_type=F32)

    d_in = []
    order = (2, 1, 3, 0)
    for dx in order:
        psend[dx] = part(other, dx).astype(BF16)
        d_in.append(go(remote(psend.at[dx], precv.at[dx], d_s.at[dx], d_r.at[dx], {"c": other})))
    o_in = []
    for n, dx in enumerate(order):
        own = part(core, dx)
        d_in[n].wait_recv()
        own = own + precv[dx].astype(F32)
        if dx:
            xsend[dx] = own.astype(BF16)
            o_in.append(go(remote(xsend.at[dx], xrecv.at[dx], o_s.at[dx], o_r.at[dx], {"x": xat(dx)})))
        else:
            pown[...] = own
    total = pown[...]
    for copy, dx in zip(o_in, order):
        copy.wait_recv()
        total = total + xrecv[dx].astype(F32)
    out[...] = total.astype(BF16)
    for copy in sent:
        copy.wait_send()


def mixed_rows(glu, q, k, v, gates, extra, taps, ln_gain, ln_bias, mem_gain, out_conv, out_mem):
    vmem = pl.BlockSpec(memory_space=pltpu.VMEM)
    hbm = pl.BlockSpec(memory_space=pltpu.HBM)
    dma = pltpu.SemaphoreType.DMA
    V = pltpu.VMEM
    return pl.pallas_call(
        mix,
        out_shape=jax.ShapeDtypeStruct((32, D), BF16),
        in_specs=[vmem] * 10 + [hbm] * 2,
        out_specs=vmem,
        scratch_shapes=[
            V((256, D), BF16), V((256, D), BF16),
            V((64, 16, 128), BF16), V((8, 128), F32),
            V((4, 16, 16, 128), BF16), V((4, 8, 128), F32),
            V((16, 16, 128), BF16), V((8, 128), F32),
            V((16, 16, 128), BF16), V((16, 8, 128), F32),
            V((16, 16, 128), BF16), V((16, 16, 128), BF16),
            V((4, 16, 16, 128), BF16), V((4, 16, 16, 128), BF16),
            V((2, 16, 256), BF16), V((2, 288, 128), F32), V((256, 256), F32),
            V((8, 256), F32), V((7, 8, 256), F32),
            V((8, 32, 256), BF16), V((8, 32, 256), BF16),
            V((256, 256), F32), V((256, 256), F32),
            V((4, 32, D), BF16), V((32, D), F32), V((4, 32, D), BF16), V((4, 32, D), BF16), V((4, 32, D), BF16),
            dma((2,)),
            dma((2,)), dma((2,)),
            dma((4,)), dma((4,)), dma((4,)), dma((4,)),
            dma((16,)), dma((16,)), dma((16,)), dma((16,)), dma((16,)), dma((16,)),
            dma((4,)), dma((4,)),
            dma((7,)), dma((7,)),
            dma((4,)), dma((4,)), dma((4,)), dma((4,)),
        ],
        compiler_params=pltpu.CompilerParams(collective_id=1, has_side_effects=True, vmem_limit_bytes=48 * 1024 * 1024),
        name="mix",
    )(glu, q, k, v, gates, extra, taps, ln_gain.reshape(1, 256), ln_bias.reshape(1, 256), mem_gain.reshape(1, 256), out_conv, out_mem)


CONV = 2048


def shards(
    tokens,
    norm_gain,
    glu_value,
    glu_gate,
    conv_taps,
    ln_gain,
    ln_bias,
    query_weight,
    key_weight,
    value_weight,
    gate_weight,
    gate_bias,
    log_decay_extra,
    mem_gain,
    out_conv,
    out_mem,
):
    glu, q, k, v, gates = projected(
        tokens, (glu_value, glu_gate, query_weight, key_weight, value_weight), norm_gain, gate_weight, gate_bias
    )
    return mixed_rows(glu, q, k, v, gates, log_decay_extra, conv_taps, ln_gain, ln_bias, mem_gain, out_conv, out_mem)


SP = ("z", "y")
TP = ("x", "c")


def solution(mesh):
    split = Mesh(mesh.devices.reshape(NZ, NY, NX, 2), ("z", "y", "x", "c"))
    placed = (
        P(SP, TP),
        P(),
        P(SP, TP),
        P(SP, TP),
        P(None, TP),
        P(TP),
        P(TP),
        P(SP, TP),
        P(SP, TP),
        P(SP, TP),
        P(),
        P(),
        P(SP, None),
        P(TP),
        P(TP, None),
        P(TP, None),
    )
    return jax.shard_map(shards, mesh=split, in_specs=placed, out_specs=P(SP + TP, None), check_vma=False)
```

time: 376 us -> 117 us (0.31)
  between operations: 104 us -> 0.17 us
  blocking collectives: 82.9 us -> 0 us
  Pallas kernels: 60.9 us -> 111 us
  other arithmetic: 27.1 us -> 0 us
  local copies, waits for them, and re-layouts: 31.4 us -> 5.32 us
  starting transfers between devices: 25.8 us -> 0 us
  waiting for transfers between devices: 19.6 us -> 0 us
  matrix products: 16.6 us -> 0 us
  loops' own time: 5.49 us -> 0 us
    pallas_call x0 -> x1, Pallas kernels: none -> 50 us  [mixed_rows(): pl.pallas_call(mix, out_shape=jax.ShapeDtypeStruct((32, D), BF16), in_spe...]
    unnamed x2 -> x0, blocking collectives: 35.7 us -> none
    all_gather x2 -> x0, blocking collectives: 29.2 us -> none  [prefix_by_axis(): pieces = jax.tree.map(lambda part: lax.all_gather(part, axis), total)]
    all_to_all x1 -> x0, starting transfers between devices: 20.4 us -> none  [sent_to_all(): return lax.all_to_all(copies, axis, split_axis=0, concat_axis=0, tiled=True)]
    all_to_all x1 -> x0, blocking collectives: 18 us -> none  [sent_and_summed(): lax.all_to_all(split_up(array, dim, length), axis, 0, 0, tiled=True)]
    dot_general x26 -> x0, matrix products: 16.6 us -> none  [the longest x2 8.86 us: finish(): jnp.einsum('htd,hde->hte', query_wide, in_mat, precision=PRECISE)]
    all_gather x4 -> x0, waiting for transfers between devices: 16.5 us -> none  [the longest x2 16.5 us: gathered_once(): both, at, found = (lax.all_gather(jnp.concatenate(lines), axis), 0, {})]
    slice x19 -> x0, local copies, waits for them, and re-layouts: 10.8 us -> none  [the longest x4 2.57 us: block_step(): carried_end = decay_sum[:, -1] + stabilizer]
  transfers between devices with their start and end apart: 7 -> 0, of which waited for: 2 -> 0; matrix products, arithmetic and copies ran while one was open for 13% -> 0% of each run, Pallas kernels for 0% -> 0%
where the time goes in v2:
time: 117 us; the launch traced here: 116 us
  Pallas kernels  111 us (95%)
  local copies, waits for them, and re-layouts  5.32 us (5%)
    pallas_call x1, Pallas kernels, projected(): pl.pallas_call(gather_project, out_shape=[jax.ShapeDtypeStruct((TOKENS, 2...  61 us
    pallas_call x1, Pallas kernels, mixed_rows(): pl.pallas_call(mix, out_shape=jax.ShapeDtypeStruct((32, D), BF16), in_spe...  50 us
    unnamed x33, local copies, waits for them, and re-layouts  5.32 us

profile of v2, /device:TPU:1, one launch (start us, length us, event | category | flops | bytes accessed | tf_op | source)
XLA Modules:
  0.0 116.5 jit_solution(2488831439870685282)
XLA Ops:
  0.0 0.0 copy-start.2
  0.0 0.0 copy-start.4
  0.0 0.0 copy-start.5
  0.0 0.0 copy-start.6
  0.0 0.0 copy-start.7
  0.0 0.0 copy-start.8
  0.0 0.0 copy-start
  0.0 1.3 %copy.17.gate_w = bf16[2048,32]{1,0:T(8,128)(2,1)S(1)} copy(bf16[2048,32]{0,1:T(8,128)(2,1)} %param.26) | data formatting | bytes 262144 | tf_op args[10]
  1.3 0.0 copy-done.2
  1.3 0.0 copy-done.4
  1.4 0.0 copy-done.5
  1.4 0.0 copy-done.6
  1.4 0.0 copy-done.7
  1.4 0.0 copy-done.8
  1.4 0.0 copy-start.9
  1.4 0.7 copy-done.9
  2.1 0.0 copy-start.13
  2.1 0.7 copy-done.13
  2.8 61.0 %gather_project.1 = (bf16[256,256]{1,0:T(8,128)(2,1)S(1)}, bf16[256,256]{1,0:T(8,128)(2,1)S(1)}, bf16[256,256]{1,0:T(8,128)(2,1)S(1)}, bf16[256,256]{1,0:T(8,128)(2,1)S(1)}, f32[256,32]{1,0:T(8,128)S(1)}) custom-call(bf16[256,256]{1,0:T(8,128)(2,1)S(1)} %copy-done.2, bf16[32,256]{1,0:T(8,128)(2,1)S(1)} %copy-done.4, bf16[32,256]{1,0:T(8,128)(2,1)S(1)} %copy-done.5, ...), custom_call_target="tpu_custom_call" | custom-call | tf_op jit(solution)/shard_map/gather_project/pallas_call | solution.py:208
  63.8 0.0 copy-done.14
  63.8 0.0 copy-start.3
  63.8 0.0 copy-start.11
  63.8 0.0 copy-start.12
  63.8 0.1 copy.18.extra
  63.9 0.0 copy-done
  63.9 0.6 copy-done.3
  64.5 0.0 copy-done.11
  64.5 0.0 copy-done.12
  64.6 0.1 copy-done.10
  64.6 1.2 %copy-done.1 = bf16[256,2048]{1,0:T(8,128)(2,1)S(1)} copy-done((bf16[256,2048]{1,0:T(8,128)(2,1)S(1)}, bf16[256,2048]{1,0:T(8,128)(2,1)}, u32[]{:S(2)}) %copy-start.1) | copy-done | bytes 1048600
  65.8 50.0 %mix.1 = bf16[32,2048]{1,0:T(8,128)(2,1)S(1)} custom-call(bf16[256,256]{1,0:T(8,128)(2,1)S(1)} %get-tuple-element.10.glu, bf16[256,256]{1,0:T(8,128)(2,1)S(1)} %get-tuple-element.11.q, bf16[256,256]{1,0:T(8,128)(2,1)S(1)} %get-tuple-element.12.k, bf16[256,256]{1,0:T(8,128)(2,1)S(1)} %get-tuple-element.13.v, f32[256,32]{1,0:T(8,128)S(1)} %get-tuple-element.14.gates, ...), custom_call_target="tpu_custom_call" | custom-call | tf_op jit(solution)/shard_map/mix/pallas_call | solution.py:542
  115.8 0.7 copy.20
  (3 shorter events, 0.0 us)
Async XLA Ops:
  0.0 1.3 %copy-start.2 = (bf16[256,256]{1,0:T(8,128)(2,1)S(1)}, bf16[256,256]{1,0:T(8,128)(2,1)}, u32[]{:S(2)}) copy-start(bf16[256,256]{1,0:T(8,128)(2,1)} %tok.1) | copy-start | bytes 393220
  0.0 1.3 %copy-start.4 = (bf16[32,256]{1,0:T(8,128)(2,1)S(1)}, bf16[32,256]{1,0:T(8,128)(2,1)}, u32[]{:S(2)}) copy-start(bf16[32,256]{1,0:T(8,128)(2,1)} %wv.1) | copy-start | bytes 49156
  0.0 1.4 %copy-start.5 = (bf16[32,256]{1,0:T(8,128)(2,1)S(1)}, bf16[32,256]{1,0:T(8,128)(2,1)}, u32[]{:S(2)}) copy-start(bf16[32,256]{1,0:T(8,128)(2,1)} %wg.1) | copy-start | bytes 49156
  0.0 1.4 %copy-start.6 = (bf16[32,256]{1,0:T(8,128)(2,1)S(1)}, bf16[32,256]{1,0:T(8,128)(2,1)}, u32[]{:S(2)}) copy-start(bf16[32,256]{1,0:T(8,128)(2,1)} %wq.1) | copy-start | bytes 49156
  0.0 1.4 %copy-start.7 = (bf16[32,256]{1,0:T(8,128)(2,1)S(1)}, bf16[32,256]{1,0:T(8,128)(2,1)}, u32[]{:S(2)}) copy-start(bf16[32,256]{1,0:T(8,128)(2,1)} %wk.1) | copy-start | bytes 49156
  0.0 1.4 %copy-start.8 = (bf16[32,256]{1,0:T(8,128)(2,1)S(1)}, bf16[32,256]{1,0:T(8,128)(2,1)}, u32[]{:S(2)}) copy-start(bf16[32,256]{1,0:T(8,128)(2,1)} %wl.1) | copy-start | bytes 49156
  0.0 63.9 %copy-start = (bf16[256,2048]{1,0:T(8,128)(2,1)S(1)}, bf16[256,2048]{1,0:T(8,128)(2,1)}, u32[]{:S(2)}) copy-start(bf16[256,2048]{1,0:T(8,128)(2,1)} %out_conv.1) | copy-start | bytes 3145732
  1.4 0.7 copy-start.9
  2.1 0.7 copy-start.13
  2.8 61.0 %copy-start.14 = (f32[256,16]{0,1:T(8,128)S(1)}, f32[256,16]{0,1:T(8,128)}, u32[]{:S(2)}) copy-start(f32[256,16]{0,1:T(8,128)} %param.28) | copy-start | bytes 49156
  63.8 0.8 copy-start.3
  63.8 0.8 copy-start.11
  63.8 0.7 copy-start.12
  63.9 0.7 copy-start.10
  64.6 1.2 %copy-start.1 = (bf16[256,2048]{1,0:T(8,128)(2,1)S(1)}, bf16[256,2048]{1,0:T(8,128)(2,1)}, u32[]{:S(2)}) copy-start(bf16[256,2048]{1,0:T(8,128)(2,1)} %out_mem.1) | copy-start | bytes 3145732

commit v3 on v2

v3 whole, which is shorter than its diff:
```python
import jax
import jax.numpy as jnp
from jax import lax
from jax.experimental import pallas as pl
from jax.experimental.pallas import tpu as pltpu
from jax.sharding import Mesh
from jax.sharding import PartitionSpec as P

MESH = pl.DeviceIdType.MESH
NZ, NY, NX = 16, 4, 4
ROWS = 32
TOKENS = 256
D = 2048
CONV = 2048
NEG = -1e30
EPS = 1e-06
F32 = jnp.float32
BF16 = jnp.bfloat16


def joined(state, level, new_state, new_level, decay):
    top = jnp.maximum(level + decay, new_level)
    early = jnp.exp(level + decay - top)
    late = jnp.exp(new_level - top)
    parts = []
    for old, new in zip(state, new_state):
        if old.ndim == 3:
            parts.append(early[None] * old + late[None] * new)
        else:
            parts.append(early * old + late * new)
    return tuple(parts), top


def log_sigmoid(x):
    return -(jnp.maximum(-x, 0.0) + jnp.log1p(jnp.exp(-jnp.abs(x))))


def ring(name, count):
    me = lax.axis_index(name)

    def at(step):
        return lax.rem(me + (step % count), count)

    return at


def remote(src, dst, ss, rs, dev):
    return pltpu.make_async_remote_copy(src, dst, ss, rs, device_id=dev, device_id_type=MESH)


GROUPS = ((2, ((6, 5),)), (4, ((11, 2), (4, 2))), (6, ((13, 2), (2, 2))), (8, ((15, 1), (0, 2))))


class ZThenY:
    def __init__(self, plan, go, w, z_sem, y_sem, z_out, y_out, base, hop, side):
        self.plan, self.go, self.w = plan, go, w
        self.z_sem, self.y_sem, self.z_out, self.y_out = z_sem, y_sem, z_out, y_out
        self.zat, self.yat = ring("z", NZ), ring("y", NY)
        self.y = lax.axis_index("y")
        self.base, self.hop, self.side = base, hop, side
        self.late = []
        self.count = 0

    def begin(self):
        for way in range(2):
            self.along(way, 1)

    def along(self, way, s):
        sign = 1 - 2 * way
        src, dst = 8 + sign * (s - 1), (8 + sign * s) % 16
        if s < 8:
            src, dst = self.w.at[src, self.y], self.w.at[dst, self.y]
        else:
            src, dst = self.w.at[src, self.y, pl.ds(16 * way, 16)], self.w.at[dst, self.y, pl.ds(16 * way, 16)]
        copy = self.go(src, dst, self.z_out, self.z_sem.at[way, s - 1], {"z": self.zat(sign)})
        now = self.base + self.hop * s

        def landed():
            copy.wait_recv()
            if s < 8:
                self.along(way, s + 1)
            if way == 1:
                for last, ranges in GROUPS:
                    if last == s:
                        for first, count in ranges:
                            self.spread(first, count, now)

        self.plan(now, landed)

    def spread(self, first, count, now):
        n = self.count
        self.count += 1
        block = self.w.at[pl.ds(first, count), self.y]
        for way in range(2):
            sign = 1 - 2 * way
            copy = self.go(block, block, self.y_out, self.y_sem.at[n, way], {"y": self.yat(sign)})

            def landed(way=way, sign=sign, copy=copy):
                copy.wait_recv()
                half = self.w.at[pl.ds(first, count), self.yat(-sign), pl.ds(16 * way, 16)]
                self.late.append(self.go(half, half, self.y_out, self.y_sem.at[n, 2 + way], {"y": self.yat(sign)}))

            self.plan(now + self.side + 0.7 * count, landed)

    def end(self):
        for copy in self.late:
            copy.wait_recv()


class YThenZ:
    def __init__(self, plan, go, w, y_sem, z_sem, out, base, hop, side):
        self.plan, self.go, self.w, self.y_sem, self.z_sem, self.out = plan, go, w, y_sem, z_sem, out
        self.zat, self.yat = ring("z", NZ), ring("y", NY)
        self.base, self.hop, self.side = base, hop, side
        self.far, self.late = [], []

    def begin(self, now):
        block = self.w.at[32 + lax.axis_index("y")]
        for way in range(2):
            sign = 1 - 2 * way
            copy = self.go(block, block, self.out, self.y_sem.at[way], {"y": self.yat(sign)})

            def landed(way=way, sign=sign, copy=copy):
                copy.wait_recv()
                half = self.w.at[32 + self.yat(-sign), pl.ds(16 * way, 16)]
                self.far.append(self.go(half, half, self.out, self.y_sem.at[2 + way], {"y": self.yat(sign)}))

            self.plan(now + self.side, landed)

    def begin_z(self):
        for copy in self.far:
            copy.wait_recv()
        for way in range(2):
            self.along(way, 1)

    def along(self, way, s):
        sign = 1 - 2 * way
        src, dst = 8 + sign * (s - 1), (8 + sign * s) % 16
        if s < 8:
            src, dst = self.w.at[pl.ds(4 * src, 4)], self.w.at[pl.ds(4 * dst, 4)]
        else:
            src, dst = self.w.at[pl.ds(4 * src + 2 * way, 2)], self.w.at[pl.ds(4 * dst + 2 * way, 2)]
        copy = self.go(src, dst, self.out, self.z_sem.at[way, s - 1], {"z": self.zat(sign)})
        if s == 8:
            self.late.append(copy)
            return

        def landed():
            copy.wait_recv()
            self.along(way, s + 1)

        self.plan(self.base + self.hop * s, landed)

    def end(self):
        for copy in self.late:
            copy.wait_recv()


def layer(
    tok, wv, wg, wq, wk, wl, gain_h, gate_h, bias_h, extra_h, taps_h, lng_h, lnb_h, memg_h, oc_h, om_h,
    out,
    w_kv, w_glu, w_q, rows_in, normed,
    gain, gate_w, gate_r, gate_b, extra, taps, ln_gain, ln_bias, mem_gain, wc, wm,
    glu, q, k, v,
    st, sm, ry, rsm, tz, gsm, rz, rgs, iz, ri, inc, rin,
    halo, ext, cv, stat, rstat, act, mem, num_f, num_b,
    psend, precv, xfar, xnear, xsum, rfar, rnear, rsum, pair,
    own, out_sem, kv_z, kv_y, glu_z, glu_y, q_y, q_z, tx_r, td_r, h_r, step_r, d_r, o_r,
):
    zat, yat, xat = ring("z", NZ), ring("y", NY), ring("x", NX)
    z, y, x, core = lax.axis_index("z"), lax.axis_index("y"), lax.axis_index("x"), lax.axis_index("c")
    other = 1 - core
    head = x * 2 + core
    sent = [0] * 12

    def go(src, dst, out_to, landed, dev):
        copy = remote(src, dst, out_sem.at[out_to], landed, dev)
        copy.start()
        size = 1
        for n in src.shape:
            size *= n
        sent[out_to] += size * jnp.dtype(src.dtype).itemsize
        return copy

    def all_of(ref, sem):
        pltpu.make_async_copy(ref, ref, sem).wait()

    def load(src, dst, n):
        copy = pltpu.make_async_copy(src, dst, own.at[n])
        copy.start()
        return copy

    l_kv = [load(src, w_kv.at[8, y, :, pl.ds(256 * n, 256)], n) for n, src in enumerate((wk, wl))]
    l_tok = load(tok, rows_in.at[head], 2)
    l_rest = [load(src, w_glu.at[8, y, :, pl.ds(256 * n, 256)], 3 + n) for n, src in enumerate((wv, wg))]
    l_q = load(wq, w_q.at[32 + y], 5)
    small = [(gain_h, gain), (gate_h, gate_w), (bias_h, gate_b), (extra_h, extra), (taps_h, taps), (lng_h, ln_gain),
             (lnb_h, ln_bias), (memg_h, mem_gain), (oc_h, wc), (om_h, wm)]
    small = [load(src, dst, 6 + n) for n, (src, dst) in enumerate(small)]

    barrier = pltpu.get_barrier_semaphore()
    greeted = [{"z": zat(1)}, {"z": zat(-1)}, {"y": yat(1)}, {"y": yat(-1)}, {"x": xat(1)}, {"x": xat(-1)}, {"c": other}]
    for dev in greeted:
        pl.semaphore_signal(barrier, inc=1, device_id=dev, device_id_type=MESH)
    pl.semaphore_wait(barrier, len(greeted))

    tasks = []
    later = {}

    def plan(when, act_on):
        tasks.append((when, len(tasks), act_on))

    def run():
        while tasks:
            item = min(tasks, key=lambda t: t[:2])
            tasks.remove(item)
            item[2]()

    for copy in l_kv:
        copy.wait()
    kv = ZThenY(plan, go, w_kv, kv_z, kv_y, 0, 1, 0.0, HOP1, SIDE1)
    kv.begin()
    values = ZThenY(plan, go, w_glu, glu_z, glu_y, 2, 3, T2, HOP2, SIDE2)
    query = YThenZ(plan, go, w_q, q_y, q_z, 4, T2, HOP2, SIDE2)

    def tokens_out():
        l_tok.wait()
        block = rows_in.at[head]
        later["tx"] = [go(block, block, 5, tx_r.at[w], {"x": xat(1 - 2 * w)}) for w in range(2)]
        later["td"] = [go(block, block, 5, td_r.at[0], {"c": other})]
        l_q.wait()
        query.begin(0.1)

    def tokens_on():
        later["tx2"] = []
        for w in range(2):
            later["tx"][w].wait_recv()
            sign = 1 - 2 * w
            slot = xat(-sign) * 2 + core
            half = rows_in.at[slot, pl.ds(128 * w, 128)]
            later["tx2"].append(go(half, half, 5, tx_r.at[2 + w], {"x": xat(sign)}))
            later["td"].append(go(rows_in.at[slot], rows_in.at[slot], 5, td_r.at[1 + w], {"c": other}))

    def tokens_far():
        slot = xat(2) * 2 + core
        for w in range(2):
            later["tx2"][w].wait_recv()
            half = rows_in.at[slot, pl.ds(128 * w, 128)]
            later["td"].append(go(half, half, 5, td_r.at[3 + w], {"c": other}))

    def tokens_in():
        for copy in later["td"]:
            copy.wait_recv()
        for copy in small:
            copy.wait()
        square = jnp.zeros((TOKENS, 256), F32)
        for b in range(8):
            wide = rows_in[b].astype(F32)
            square = square + wide * wide
        scale = lax.rsqrt(jnp.sum(square, axis=1, keepdims=True) / D + EPS)
        for p in range(16):
            at_z = zat(8 - p)
            cols = pl.ds(pl.multiple_of(at_z * 128, 128), 128)
            part = rows_in[at_z // 2, :, pl.ds(pl.multiple_of((at_z % 2) * 128, 128), 128)].astype(F32)
            normed[:, 128 * p : 128 * p + 128] = (part * scale * gain[:, cols]).astype(BF16)
            gate_r[:, 128 * p : 128 * p + 128] = gate_w[:, cols]

    plan(0.0, tokens_out)
    plan(3.5, tokens_on)
    plan(7.0, tokens_far)
    plan(10.1, tokens_in)

    sub = lax.broadcasted_iota(jnp.int32, (32, TOKENS), 0)
    sub16 = lax.broadcasted_iota(jnp.int32, (16, TOKENS), 0)
    t_at = lax.broadcasted_iota(jnp.int32, (TOKENS, TOKENS), 0)
    s_at = lax.broadcasted_iota(jnp.int32, (TOKENS, TOKENS), 1)

    def as_row(col):
        return jnp.sum(jnp.where(t_at == s_at, col, 0.0), axis=0, keepdims=True)

    def as_column(row):
        return jnp.sum(jnp.where(t_at == s_at, row, 0.0), axis=1, keepdims=True)

    def ends(total, sum_row, gate):
        to_end = total - sum_row + gate
        level = jnp.max(to_end, axis=1, keepdims=True)
        return as_column(jnp.exp(to_end - level) * 0.0625), level

    def gates_in():
        diagonal = lax.broadcasted_iota(jnp.int32, (32, 32), 0) == lax.broadcasted_iota(jnp.int32, (32, 32), 1)
        bias = jnp.sum(jnp.where(diagonal, gate_b[...], 0.0), axis=1, keepdims=True)
        gates = lax.dot_general(gate_r[...], normed[...], (((1,), (1,)), ((), ())), preferred_element_type=F32) + bias

        def gate_row(n):
            return jnp.sum(jnp.where(sub == 8 * n + head, gates, 0.0), axis=0, keepdims=True)

        def extra_row(n):
            return jnp.sum(jnp.where(sub16 == 8 * n + head, extra[...], 0.0), axis=0, keepdims=True)

        later["rows"] = gate_row(0), gate_row(2)
        lf_f = log_sigmoid(gate_row(1)) + extra_row(0)
        lf_b = log_sigmoid(gate_row(3)) + extra_row(1)
        sum_f = jnp.sum(jnp.where(s_at <= t_at, lf_f, 0.0), axis=1, keepdims=True)
        sum_b = jnp.sum(jnp.where(s_at >= t_at, lf_b, 0.0), axis=1, keepdims=True)
        sum_f_row, sum_b_row = as_row(sum_f), as_row(sum_b)
        later["sums"] = sum_f, sum_f_row, sum_b, sum_b_row
        total_f = jnp.sum(lf_f, axis=1, keepdims=True)
        total_b = jnp.sum(lf_b, axis=1, keepdims=True)
        end_f, level_f = ends(total_f, sum_f_row, later["rows"][0])
        end_b, level_b = ends(total_b, sum_b_row, later["rows"][1])
        later["ends"] = end_f, end_b
        for n, one in enumerate((total_f, level_f, total_b, level_b)):
            sm[4 + n : 5 + n, :] = jnp.broadcast_to(one, (1, 128))

    plan(12.1, gates_in)

    def rest_out():
        for copy in l_rest:
            copy.wait()
        values.begin()
        query.begin_z()

    plan(T2, rest_out)

    def project(w, n):
        return jnp.dot(normed[...], w[:, :, :, 256 * n : 256 * n + 256].reshape(D, 256), preferred_element_type=F32)

    def states_out():
        kv.end()
        v[...] = project(w_kv, 1).astype(BF16)
        keys = project(w_kv, 0).astype(BF16)
        k[...] = keys
        keys = keys.astype(F32)

        def summary(end):
            weighted = keys * end
            state = lax.dot_general(weighted.astype(BF16), v[...], (((0,), (0,)), ((), ())), preferred_element_type=F32)
            return state, jnp.sum(weighted, axis=0, keepdims=True)

        state_f, vec_f = summary(later["ends"][0])
        state_b, vec_b = summary(later["ends"][1])
        for h in range(2):
            cols = slice(128 * h, 128 * h + 128)
            both = jnp.concatenate([state_f[:, cols].reshape(32, 8, 128), state_b[:, cols].reshape(32, 8, 128)], axis=1)
            st[32 * h : 32 * h + 32] = both.astype(BF16)
        for n, row in enumerate((vec_f[:, :128], vec_f[:, 128:], vec_b[:, :128], vec_b[:, 128:])):
            sm[n : n + 1, :] = row
        ry[y] = st[pl.ds(y * 16, 16)]
        rsm[y] = sm[...]
        for dy in (2, 1, 3):
            to = yat(dy)
            go(sm, rsm.at[y], 6, step_r.at[0], {"y": to})
            go(st.at[pl.ds(to * 16, 16)], ry.at[y], 6, step_r.at[1], {"y": to})

    plan(TS, states_out)

    def y_pieces(n, d):
        return ry[n].astype(F32)[:, 8 * d : 8 * d + 8, :], rsm[n, 2 * d : 2 * d + 2, :]

    def y_scalars(n, d):
        return rsm[n, 5 + 2 * d : 6 + 2 * d, :], rsm[n, 4 + 2 * d : 5 + 2 * d, :]

    def y_walk(d, start, level):
        state = start
        found = []
        for n in range(NY) if d == 0 else reversed(range(NY)):
            found.append((n, state, level))
            state, level = joined(state, level, y_pieces(n, d), *y_scalars(n, d))
        return found, state, level

    low = jnp.full((1, 128), NEG, F32)
    far_first = (8, 7, 9, 6, 10, 5, 11, 4, 12, 3, 13, 2, 14, 1, 15)

    def groups_out():
        all_of(rsm.at[pl.ds(0, 3)], step_r.at[0])
        all_of(ry.at[pl.ds(0, 3)], step_r.at[1])
        zero = (jnp.zeros((16, 8, 128), F32), jnp.zeros((2, 128), F32))
        groups = []
        for d in range(2):
            _, group, level = y_walk(d, zero, low)
            groups.append(group)
            gsm[2 * d : 2 * d + 2, :] = group[1]
            decay = low * 0.0
            for n in range(NY):
                decay = decay + y_scalars(n, d)[1]
            gsm[4 + 2 * d : 5 + 2 * d, :] = decay
            gsm[5 + 2 * d : 6 + 2 * d, :] = level
        tz[...] = jnp.concatenate([groups[0][0], groups[1][0]], axis=1).astype(BF16)
        rz[z] = tz[z]
        rgs[z] = gsm[...]
        for dz in far_first:
            to = zat(dz)
            go(tz.at[to], rz.at[z], 10, step_r.at[2], {"z": to})
            go(gsm, rgs.at[z], 10, step_r.at[3], {"z": to})

    plan(TY, groups_out)

    def pieces_back():
        all_of(rz.at[pl.ds(0, 15)], step_r.at[2])
        all_of(rgs.at[pl.ds(0, 15)], step_r.at[3])
        later["came"], later["came_level"] = [], []
        entering = []
        for d in range(2):
            state = (jnp.zeros((8, 128), F32), jnp.zeros((2, 128), F32))
            level = low
            kept, kept_level = jnp.zeros((2, 128), F32), low
            lines = [None] * NZ
            for n in range(NZ) if d == 0 else reversed(range(NZ)):
                lines[n] = state[0]
                kept = jnp.where(z == n, state[1], kept)
                kept_level = jnp.where(z == n, level, kept_level)
                piece = (rz[n].astype(F32)[8 * d : 8 * d + 8, :], rgs[n, 2 * d : 2 * d + 2, :])
                state, level = joined(state, level, piece, rgs[n, 5 + 2 * d : 6 + 2 * d, :], rgs[n, 4 + 2 * d : 5 + 2 * d, :])
            entering.append(lines)
            later["came"].append(kept)
            later["came_level"].append(kept_level)
        for n in range(NZ):
            iz[n] = jnp.concatenate([entering[0][n], entering[1][n]], axis=0).astype(BF16)
        ri[z] = iz[z]
        for dz in far_first:
            to = zat(dz)
            go(iz.at[to], ri.at[z], 10, step_r.at[4], {"z": to})

    plan(TZ, pieces_back)
    run()
    query.end()
    q[...] = jnp.dot(normed[...], w_q[...].reshape(D, 256), preferred_element_type=F32).astype(BF16)
    values.end()
    glu[...] = (project(w_glu, 0) * jax.nn.sigmoid(project(w_glu, 1))).astype(BF16)
    in_f_row, in_b_row = later["rows"]
    sum_f, sum_f_row, sum_b, sum_b_row = later["sums"]
    after = {"z": zat(lax.convert_element_type(y == NY - 1, jnp.int32)), "y": yat(1)}
    before = {"z": lax.rem(z + NZ - lax.convert_element_type(y == 0, jnp.int32), NZ), "y": yat(-1)}
    halos = [
        go(glu.at[pl.ds(240, 16), :], halo.at[0], 11, h_r.at[0], after),
        go(glu.at[pl.ds(0, 16), :], halo.at[1], 11, h_r.at[1], before),
    ]

    scores = lax.dot_general(q[...], k[...], (((1,), (1,)), ((), ())), preferred_element_type=F32) * 0.0625

    def inside(mask, sums, sum_row, gate_at, numerator):
        log_weight = jnp.where(mask, sums - sum_row + gate_at, NEG)
        top = jnp.max(log_weight, axis=1, keepdims=True)
        weights = scores * jnp.exp(log_weight - top)
        numerator[...] = jnp.dot(weights.astype(BF16), v[...], preferred_element_type=F32)
        return jnp.sum(weights, axis=1, keepdims=True), top

    den_f, top_f = inside(s_at <= t_at, sum_f, sum_f_row, in_f_row, num_f)

    all_of(ri.at[pl.ds(0, 15)], step_r.at[4])
    back = [None] * 2
    kept_vec = []
    for d in range(2):
        start = (ri[...].astype(F32)[:, 8 * d : 8 * d + 8, :], later["came"][d])
        found, _, _ = y_walk(d, start, later["came_level"][d])
        kept, kept_level = jnp.zeros((2, 128), F32), low
        back[d] = [None] * NY
        for n, state, level in found:
            back[d][n] = state[0]
            kept = jnp.where(y == n, state[1], kept)
            kept_level = jnp.where(y == n, level, kept_level)
        kept_vec.append((kept, kept_level))
    for n in range(NY):
        inc[n] = jnp.concatenate([back[0][n], back[1][n]], axis=1).astype(BF16)
    rin[y] = inc[y]
    for dy in (2, 1, 3):
        to = yat(dy)
        go(inc.at[to], rin.at[y], 9, step_r.at[5], {"y": to})
    for copy in halos:
        copy.wait_recv()
    place = z * NY + y
    for h in range(2):
        cols = slice(128 * h, 128 * h + 128)
        ext[h, 0:16, :] = jnp.where(place == 0, 0.0, halo[0][:, cols].astype(F32))
        ext[h, 16:272, :] = glu[:, cols].astype(F32)
        ext[h, 272:288, :] = jnp.where(place == NZ * NY - 1, 0.0, halo[1][:, cols].astype(F32))
    for h in range(2):
        cols = slice(128 * h, 128 * h + 128)

        def rows_of(n, carry):
            start = n * 64
            total = jnp.zeros((64, 128), F32)
            for j in range(31):
                total = total + taps[j : j + 1, cols] * ext[h, pl.ds(start + (j + 1), 64), :]
            cv[pl.ds(pl.multiple_of(start, 64), 64), cols] = total
            return carry

        lax.fori_loop(0, 4, rows_of, 0)
    conv = cv[...]
    stat[0:1, :] = as_row(jnp.sum(conv, axis=1, keepdims=True))
    stat[1:2, :] = as_row(jnp.sum(conv * conv, axis=1, keepdims=True))
    stat[2:8, :] = jnp.zeros((6, TOKENS), F32)
    tp_peers = [(dx, cc) for dx in range(NX) for cc in range(2) if dx or cc]
    for n, (dx, cc) in enumerate(tp_peers):
        dev = {"x": xat(dx), "c": core if cc == 0 else other}
        go(stat, rstat.at[n], 11, step_r.at[6], dev)
    den_b, top_b = inside(s_at >= t_at, sum_b, sum_b_row, in_b_row, num_b)

    all_of(rin.at[pl.ds(0, 3)], step_r.at[5])

    def finished(d, numerator, den, top, sums):
        vec, level = kept_vec[d]
        vec = jnp.concatenate([vec[0:1, :], vec[1:2, :]], axis=1)
        state = rin[...].reshape(64, 16, 128).astype(F32)[:, 8 * d : 8 * d + 8, :]
        left = state[:32].reshape(256, 128).astype(BF16)
        right = state[32:].reshape(256, 128).astype(BF16)
        carried = sums + level[:, 0:1]
        high = jnp.maximum(top, carried)
        near = jnp.exp(top - high)
        far = jnp.exp(carried - high)
        read = jnp.concatenate(
            [jnp.dot(q[...], left, preferred_element_type=F32), jnp.dot(q[...], right, preferred_element_type=F32)], axis=1
        )
        upper = near * numerator[...] + far * read
        lower = near * den + far * jnp.sum(q[...].astype(F32) * vec, axis=1, keepdims=True)
        return upper / jnp.maximum(jnp.abs(lower), jnp.exp(-high))

    summed = finished(0, num_f, den_f, top_f, sum_f) + finished(1, num_b, den_b, top_b, sum_b)
    scale = lax.rsqrt(jnp.mean(summed * summed, axis=1, keepdims=True) + EPS)
    heads = (summed * scale * mem_gain[...]).astype(BF16).reshape(4, 2, 32, 256)
    mem[0] = heads[:, 0]
    mem[1] = heads[:, 1]

    sums = stat[...]
    all_of(rstat, step_r.at[6])
    for n in range(7):
        sums = sums + rstat[n]
    mean = as_column(sums[0:1, :]) / CONV
    var = as_column(sums[1:2, :]) / CONV - mean * mean
    normal = (cv[...] - mean) * lax.rsqrt(var + EPS) * ln_gain[...] + ln_bias[...]
    gated = (normal * jax.nn.sigmoid(normal)).astype(BF16).reshape(4, 2, 32, 256)
    act[0] = gated[:, 0]
    act[1] = gated[:, 1]

    def part(c, h):
        cols = slice(1024 * h, 1024 * h + 1024)
        rows = jnp.dot(act[c].reshape(128, 256), wc[:, cols], preferred_element_type=F32)
        return (rows + jnp.dot(mem[c].reshape(128, 256), wm[:, cols], preferred_element_type=F32)).reshape(4, 32, 1024)

    d_in = []
    for h in range(2):
        psend[h] = part(other, h).astype(BF16)
        d_in.append(go(psend.at[h], precv.at[h], 7, d_r.at[h], {"c": other}))
    o_in = []
    for h in range(2):
        pair[...] = part(core, h)
        d_in[h].wait_recv()
        pair[...] = pair[...] + precv[h].astype(F32)
        sign = 1 - 2 * h
        xfar[h] = pair[xat(2)].astype(BF16)
        xnear[h] = pair[xat(-sign)].astype(BF16)
        far = go(xfar.at[h], rfar.at[h], 8, o_r.at[0, h], {"x": xat(sign)})
        near = go(xnear.at[h], rnear.at[h], 8, o_r.at[1, h], {"x": xat(-sign)})
        o_in.append((far, near))
        psum = pair[xat(sign)]
        rest = pair[x]
        if h == 0:
            held = psum, rest
    both = [held, (psum, rest)]
    last = []
    for h in range(2):
        sign = 1 - 2 * h
        o_in[h][0].wait_recv()
        xsum[h] = (both[h][0] + rfar[h].astype(F32)).astype(BF16)
        last.append(go(xsum.at[h], rsum.at[h], 8, o_r.at[2, h], {"x": xat(sign)}))
    for h in range(2):
        o_in[h][1].wait_recv()
        last[h].wait_recv()
        out[:, 1024 * h : 1024 * h + 1024] = (both[h][1] + rnear[h].astype(F32) + rsum[h].astype(F32)).astype(BF16)
    for n, size in enumerate(sent):
        if size > 1024 * 1024:
            count, same = size // 131072, w_kv
        elif size > 256 * 1024:
            count, same = size // 16384, w_q
        else:
            count, same = size // 4096, st
        assert size % count == 0
        all_of(same.at[pl.ds(0, count)], out_sem.at[n])


SP = ("z", "y")
TP = ("x", "c")


def shards(
    tokens, norm_gain, glu_value, glu_gate, conv_taps, ln_gain, ln_bias, query_weight, key_weight, value_weight,
    gate_weight, gate_bias, log_decay_extra, mem_gain, out_conv, out_mem,
):
    hbm = pl.BlockSpec(memory_space=pltpu.HBM)
    dma = pltpu.SemaphoreType.DMA
    V = pltpu.VMEM
    return pl.pallas_call(
        layer,
        out_shape=jax.ShapeDtypeStruct((32, D), BF16),
        in_specs=[hbm] * 16,
        out_specs=pl.BlockSpec(memory_space=pltpu.VMEM),
        scratch_shapes=[
            V((16, 4, ROWS, 512), BF16), V((16, 4, ROWS, 512), BF16), V((64, ROWS, 256), BF16),
            V((8, TOKENS, 256), BF16), V((TOKENS, D), BF16),
            V((1, D), F32), V((32, D), BF16), V((32, D), BF16), V((1, 32), F32), V((16, TOKENS), F32), V((31, 256), F32),
            V((1, 256), F32), V((1, 256), F32), V((1, 256), F32), V((256, D), BF16), V((256, D), BF16),
            V((TOKENS, 256), BF16), V((TOKENS, 256), BF16), V((TOKENS, 256), BF16), V((TOKENS, 256), BF16),
            V((64, 16, 128), BF16), V((8, 128), F32),
            V((4, 16, 16, 128), BF16), V((4, 8, 128), F32),
            V((16, 16, 128), BF16), V((8, 128), F32),
            V((16, 16, 128), BF16), V((16, 8, 128), F32),
            V((16, 16, 128), BF16), V((16, 16, 128), BF16),
            V((4, 16, 16, 128), BF16), V((4, 16, 16, 128), BF16),
            V((2, 16, 256), BF16), V((2, 288, 128), F32), V((256, 256), F32),
            V((8, 256), F32), V((7, 8, 256), F32),
            V((2, 4, 32, 256), BF16), V((2, 4, 32, 256), BF16),
            V((256, 256), F32), V((256, 256), F32),
            V((2, 4, 32, 1024), BF16), V((2, 4, 32, 1024), BF16),
            V((2, 32, 1024), BF16), V((2, 32, 1024), BF16), V((2, 32, 1024), BF16),
            V((2, 32, 1024), BF16), V((2, 32, 1024), BF16), V((2, 32, 1024), BF16),
            V((4, 32, 1024), F32),
            dma((16,)), dma((12,)),
            dma((2, 8)), dma((7, 4)), dma((2, 8)), dma((7, 4)), dma((4,)), dma((2, 8)),
            dma((4,)), dma((5,)), dma((2,)), dma((7,)), dma((2,)), dma((3, 2)),
        ],
        compiler_params=pltpu.CompilerParams(collective_id=0, has_side_effects=True, vmem_limit_bytes=VMEM_BYTES),
        name="layer",
    )(
        tokens, glu_value, glu_gate, query_weight, key_weight, value_weight,
        norm_gain.reshape(1, D), gate_weight.T, gate_bias.reshape(1, 32), log_decay_extra.T, conv_taps,
        ln_gain.reshape(1, 256), ln_bias.reshape(1, 256), mem_gain.reshape(1, 256), out_conv, out_mem,
    )


VMEM_BYTES = 60 * 1024 * 1024
HOP1, SIDE1, HOP2, SIDE2 = 2.3, 2.0, 3.2, 2.2
T2, TS, TY, TZ = 16.0, 26.0, 32.5, 41.0


def solution(mesh):
    split = Mesh(mesh.devices.reshape(NZ, NY, NX, 2), ("z", "y", "x", "c"))
    placed = (
        P(SP, TP), P(), P(SP, TP), P(SP, TP), P(None, TP), P(TP), P(TP), P(SP, TP), P(SP, TP), P(SP, TP),
        P(), P(), P(SP, None), P(TP), P(TP, None), P(TP, None),
    )
    return jax.shard_map(shards, mesh=split, in_specs=placed, out_specs=P(SP + TP, None), check_vma=False)
```

time: 117 us -> 99.7 us (0.85)
  Pallas kernels: 111 us -> 97.7 us
  local copies, waits for them, and re-layouts: 5.32 us -> 1.57 us
    pallas_call x2 -> x1, Pallas kernels: 111 us -> 97.7 us  [shards(): pl.pallas_call(layer, out_shape=jax.ShapeDtypeStruct((32, D), BF16), in_s...]
    unnamed x33 -> x1, local copies, waits for them, and re-layouts: 5.32 us -> 1.57 us
where the time goes in v3:
time: 99.7 us; the launch traced here: 99.3 us
  Pallas kernels  97.7 us (98%)
  local copies, waits for them, and re-layouts  1.57 us (2%)
    pallas_call x1, Pallas kernels, shards(): pl.pallas_call(layer, out_shape=jax.ShapeDtypeStruct((32, D), BF16), in_s...  97.7 us

profile of v3, /device:TPU:1, one launch (start us, length us, event | category | flops | bytes accessed | tf_op | source)
XLA Modules:
  0.0 99.3 jit_solution(16097959253186478641)
XLA Ops:
  0.0 97.7 %layer.1 = bf16[32,2048]{1,0:T(8,128)(2,1)} custom-call(bf16[256,256]{1,0:T(8,128)(2,1)} %tok.1, bf16[32,256]{1,0:T(8,128)(2,1)} %wv.1, bf16[32,256]{1,0:T(8,128)(2,1)} %wg.1, bf16[32,256]{1,0:T(8,128)(2,1)} %wq.1, bf16[32,256]{1,0:T(8,128)(2,1)} %wk.1, bf16[32,256]{1,0:T(8,128)(2,1)} %wl.1, f32[1,2048]{1,0:T(1,128)} %bitcast.9, bf16[32,2048]{1,0:T(8,128)(2,1)} %bitcast.7, ...), custom_call_target="tpu_custom_call" | custom-call | tf_op jit(solution)/shard_map/layer/pallas_call | solution.py:592
  97.7 1.6 %copy.18 = bf16[32,2048]{1,0:T(8,128)(2,1)} copy(bf16[32,2048]{1,0:T(8,128)(2,1)} %layer.1) | data formatting | bytes 262144

commit v4 on v3

--- a/solution.py
+++ b/solution.py
@@ -48,12 +48,22 @@
     return pltpu.make_async_remote_copy(src, dst, ss, rs, device_id=dev, device_id_type=MESH)
 
 
-GROUPS = ((2, ((6, 5),)), (4, ((11, 2), (4, 2))), (6, ((13, 2), (2, 2))), (8, ((15, 1), (0, 2))))
+SEED = 5
+GROUPS = ((2, ((6, 5),)), (4, ((11, 4), (2, 4))), (8, ((15, 1), (0, 2))))
+
+
+def step_of(sign, s):
+    fresh = s in (1, SEED)
+    return (8 if fresh else 8 + sign * (s - 1)), (8 + sign * s) % 16, s if fresh else 1
+
+
+def time_of(s, hop, seed):
+    return hop * s if s < SEED else seed + hop * (s - SEED)
 
 
 class ZThenY:
-    def __init__(self, plan, go, w, z_sem, y_sem, z_out, y_out, base, hop, side):
-        self.plan, self.go, self.w = plan, go, w
+    def __init__(self, plan, go, w, z_sem, y_sem, z_out, y_out, base, hop, seed, side):
+        self.plan, self.go, self.w, self.seed = plan, go, w, seed
         self.z_sem, self.y_sem, self.z_out, self.y_out = z_sem, y_sem, z_out, y_out
         self.zat, self.yat = ring("z", NZ), ring("y", NY)
         self.y = lax.axis_index("y")
@@ -62,22 +72,23 @@
         self.count = 0
 
     def begin(self):
-        for way in range(2):
-            self.along(way, 1)
+        for s in (SEED, 1):
+            for way in range(2):
+                self.along(way, s)
 
     def along(self, way, s):
         sign = 1 - 2 * way
-        src, dst = 8 + sign * (s - 1), (8 + sign * s) % 16
+        src, dst, away = step_of(sign, s)
         if s < 8:
             src, dst = self.w.at[src, self.y], self.w.at[dst, self.y]
         else:
             src, dst = self.w.at[src, self.y, pl.ds(16 * way, 16)], self.w.at[dst, self.y, pl.ds(16 * way, 16)]
-        copy = self.go(src, dst, self.z_out, self.z_sem.at[way, s - 1], {"z": self.zat(sign)})
-        now = self.base + self.hop * s
+        copy = self.go(src, dst, self.z_out, self.z_sem.at[way, s - 1], {"z": self.zat(sign * away)})
+        now = self.base + time_of(s, self.hop, self.seed)
 
         def landed():
             copy.wait_recv()
-            if s < 8:
+            if s not in (SEED - 1, 8):
                 self.along(way, s + 1)
             if way == 1:
                 for last, ranges in GROUPS:
@@ -108,7 +119,8 @@
 
 
 class YThenZ:
-    def __init__(self, plan, go, w, y_sem, z_sem, out, base, hop, side):
+    def __init__(self, plan, go, w, y_sem, z_sem, out, base, hop, seed, side):
+        self.seed = seed
         self.plan, self.go, self.w, self.y_sem, self.z_sem, self.out = plan, go, w, y_sem, z_sem, out
         self.zat, self.yat = ring("z", NZ), ring("y", NY)
         self.base, self.hop, self.side = base, hop, side
@@ -130,17 +142,18 @@
     def begin_z(self):
         for copy in self.far:
             copy.wait_recv()
-        for way in range(2):
-            self.along(way, 1)
+        for s in (SEED, 1):
+            for way in range(2):
+                self.along(way, s)
 
     def along(self, way, s):
         sign = 1 - 2 * way
-        src, dst = 8 + sign * (s - 1), (8 + sign * s) % 16
+        src, dst, away = step_of(sign, s)
         if s < 8:
             src, dst = self.w.at[pl.ds(4 * src, 4)], self.w.at[pl.ds(4 * dst, 4)]
         else:
             src, dst = self.w.at[pl.ds(4 * src + 2 * way, 2)], self.w.at[pl.ds(4 * dst + 2 * way, 2)]
-        copy = self.go(src, dst, self.out, self.z_sem.at[way, s - 1], {"z": self.zat(sign)})
+        copy = self.go(src, dst, self.out, self.z_sem.at[way, s - 1], {"z": self.zat(sign * away)})
         if s == 8:
             self.late.append(copy)
             return
@@ -149,7 +162,10 @@
             copy.wait_recv()
             self.along(way, s + 1)
 
-        self.plan(self.base + self.hop * s, landed)
+        if s == SEED - 1:
+            self.late.append(copy)
+            return
+        self.plan(self.base + time_of(s, self.hop, self.seed), landed)
 
     def end(self):
         for copy in self.late:
@@ -199,7 +215,7 @@
     small = [load(src, dst, 6 + n) for n, (src, dst) in enumerate(small)]
 
     barrier = pltpu.get_barrier_semaphore()
-    greeted = [{"z": zat(1)}, {"z": zat(-1)}, {"y": yat(1)}, {"y": yat(-1)}, {"x": xat(1)}, {"x": xat(-1)}, {"c": other}]
+    greeted = [{"z": zat(1)}, {"z": zat(-1)}, {"z": zat(SEED)}, {"z": zat(-SEED)}, {"y": yat(1)}, {"y": yat(-1)}, {"x": xat(1)}, {"x": xat(-1)}, {"c": other}]
     for dev in greeted:
         pl.semaphore_signal(barrier, inc=1, device_id=dev, device_id_type=MESH)
     pl.semaphore_wait(barrier, len(greeted))
@@ -218,10 +234,10 @@
 
     for copy in l_kv:
         copy.wait()
-    kv = ZThenY(plan, go, w_kv, kv_z, kv_y, 0, 1, 0.0, HOP1, SIDE1)
+    kv = ZThenY(plan, go, w_kv, kv_z, kv_y, 0, 1, 0.0, HOP1, SEED1, SIDE1)
     kv.begin()
-    values = ZThenY(plan, go, w_glu, glu_z, glu_y, 2, 3, T2, HOP2, SIDE2)
-    query = YThenZ(plan, go, w_q, q_y, q_z, 4, T2, HOP2, SIDE2)
+    values = ZThenY(plan, go, w_glu, glu_z, glu_y, 2, 3, T2, HOP2, SEED2, SIDE2)
+    query = YThenZ(plan, go, w_q, q_y, q_z, 4, T2, HOP3, SEED3, SIDE2)
 
     def tokens_out():
         l_tok.wait()
@@ -615,7 +631,7 @@
             V((2, 32, 1024), BF16), V((2, 32, 1024), BF16), V((2, 32, 1024), BF16),
             V((4, 32, 1024), F32),
             dma((16,)), dma((12,)),
-            dma((2, 8)), dma((7, 4)), dma((2, 8)), dma((7, 4)), dma((4,)), dma((2, 8)),
+            dma((2, 8)), dma((5, 4)), dma((2, 8)), dma((5, 4)), dma((4,)), dma((2, 8)),
             dma((4,)), dma((5,)), dma((2,)), dma((7,)), dma((2,)), dma((3, 2)),
         ],
         compiler_params=pltpu.CompilerParams(collective_id=0, has_side_effects=True, vmem_limit_bytes=VMEM_BYTES),
@@ -627,9 +643,10 @@
     )
 
 
-VMEM_BYTES = 60 * 1024 * 1024
-HOP1, SIDE1, HOP2, SIDE2 = 2.3, 2.0, 3.2, 2.2
-T2, TS, TY, TZ = 16.0, 26.0, 32.5, 41.0
+VMEM_BYTES = 66700000
+HOP1, SEED1, SIDE1 = 3.0, 6.1, 2.6
+HOP2, SEED2, HOP3, SEED3, SIDE2 = 6.0, 10.0, 6.8, 11.0, 2.6
+T2, TS, TY, TZ = 12.5, 27.5, 33.5, 41.5
 
 
 def solution(mesh):

time: 99.7 us -> 94.4 us (0.947)
  Pallas kernels: 97.7 us -> 92.6 us
    pallas_call x1, Pallas kernels: 97.7 us -> 92.6 us  [shards(): pl.pallas_call(layer, out_shape=jax.ShapeDtypeStruct((32, D), BF16), in_s...]
where the time goes in v4:
time: 94.4 us; the launch traced here: 94.2 us
  Pallas kernels  92.6 us (98%)
  local copies, waits for them, and re-layouts  1.57 us (2%)
    pallas_call x1, Pallas kernels, shards(): pl.pallas_call(layer, out_shape=jax.ShapeDtypeStruct((32, D), BF16), in_s...  92.6 us

profile of v4, /device:TPU:1, one launch (start us, length us, event | category | flops | bytes accessed | tf_op | source)
XLA Modules:
  0.0 94.2 jit_solution(14857437562576024520)
XLA Ops:
  0.0 92.6 %layer.1 = bf16[32,2048]{1,0:T(8,128)(2,1)} custom-call(bf16[256,256]{1,0:T(8,128)(2,1)} %tok.1, bf16[32,256]{1,0:T(8,128)(2,1)} %wv.1, bf16[32,256]{1,0:T(8,128)(2,1)} %wg.1, bf16[32,256]{1,0:T(8,128)(2,1)} %wq.1, bf16[32,256]{1,0:T(8,128)(2,1)} %wk.1, bf16[32,256]{1,0:T(8,128)(2,1)} %wl.1, f32[1,2048]{1,0:T(1,128)} %bitcast.9, bf16[32,2048]{1,0:T(8,128)(2,1)} %bitcast.7, ...), custom_call_target="tpu_custom_call" | custom-call | tf_op jit(solution)/shard_map/layer/pallas_call | solution.py:608
  92.6 1.6 %copy.18 = bf16[32,2048]{1,0:T(8,128)(2,1)} copy(bf16[32,2048]{1,0:T(8,128)(2,1)} %layer.1) | data formatting | bytes 262144

commit v5 on v4

--- a/solution.py
+++ b/solution.py
@@ -328,7 +328,7 @@
         for n, one in enumerate((total_f, level_f, total_b, level_b)):
             sm[4 + n : 5 + n, :] = jnp.broadcast_to(one, (1, 128))
 
-    plan(12.1, gates_in)
+    plan(12.6, gates_in)
 
     def rest_out():
         for copy in l_rest:
@@ -566,21 +566,21 @@
         xfar[h] = pair[xat(2)].astype(BF16)
         xnear[h] = pair[xat(-sign)].astype(BF16)
         far = go(xfar.at[h], rfar.at[h], 8, o_r.at[0, h], {"x": xat(sign)})
-        near = go(xnear.at[h], rnear.at[h], 8, o_r.at[1, h], {"x": xat(-sign)})
-        o_in.append((far, near))
+        o_in.append(far)
         psum = pair[xat(sign)]
         rest = pair[x]
         if h == 0:
             held = psum, rest
     both = [held, (psum, rest)]
+    near = [go(xnear.at[h], rnear.at[h], 8, o_r.at[1, h], {"x": xat(2 * h - 1)}) for h in range(2)]
     last = []
     for h in range(2):
         sign = 1 - 2 * h
-        o_in[h][0].wait_recv()
+        o_in[h].wait_recv()
         xsum[h] = (both[h][0] + rfar[h].astype(F32)).astype(BF16)
         last.append(go(xsum.at[h], rsum.at[h], 8, o_r.at[2, h], {"x": xat(sign)}))
     for h in range(2):
-        o_in[h][1].wait_recv()
+        near[h].wait_recv()
         last[h].wait_recv()
         out[:, 1024 * h : 1024 * h + 1024] = (both[h][1] + rnear[h].astype(F32) + rsum[h].astype(F32)).astype(BF16)
     for n, size in enumerate(sent):
@@ -646,7 +646,7 @@
 VMEM_BYTES = 66700000
 HOP1, SEED1, SIDE1 = 3.0, 6.1, 2.6
 HOP2, SEED2, HOP3, SEED3, SIDE2 = 6.0, 10.0, 6.8, 11.0, 2.6
-T2, TS, TY, TZ = 12.5, 27.5, 33.5, 41.5
+T2, TS, TY, TZ = 12.5, 27.5, 33.5, 42.0
 
 
 def solution(mesh):

time: 94.4 us -> 93.3 us (0.988)
  Pallas kernels: 92.6 us -> 91.1 us
    pallas_call x1, Pallas kernels: 92.6 us -> 91.1 us  [shards(): pl.pallas_call(layer, out_shape=jax.ShapeDtypeStruct((32, D), BF16), in_s...]
where the time goes in v5:
time: 93.3 us; the launch traced here: 92.7 us
  Pallas kernels  91.1 us (98%)
  local copies, waits for them, and re-layouts  1.57 us (2%)
    pallas_call x1, Pallas kernels, shards(): pl.pallas_call(layer, out_shape=jax.ShapeDtypeStruct((32, D), BF16), in_s...  91.1 us

profile of v5, /device:TPU:1, one launch (start us, length us, event | category | flops | bytes accessed | tf_op | source)
XLA Modules:
  0.0 92.7 jit_solution(3532504394133748587)
XLA Ops:
  0.0 91.1 %layer.1 = bf16[32,2048]{1,0:T(8,128)(2,1)} custom-call(bf16[256,256]{1,0:T(8,128)(2,1)} %tok.1, bf16[32,256]{1,0:T(8,128)(2,1)} %wv.1, bf16[32,256]{1,0:T(8,128)(2,1)} %wg.1, bf16[32,256]{1,0:T(8,128)(2,1)} %wq.1, bf16[32,256]{1,0:T(8,128)(2,1)} %wk.1, bf16[32,256]{1,0:T(8,128)(2,1)} %wl.1, f32[1,2048]{1,0:T(1,128)} %bitcast.9, bf16[32,2048]{1,0:T(8,128)(2,1)} %bitcast.7, ...), custom_call_target="tpu_custom_call" | custom-call | tf_op jit(solution)/shard_map/layer/pallas_call | solution.py:608
  91.1 1.6 %copy.18 = bf16[32,2048]{1,0:T(8,128)(2,1)} copy(bf16[32,2048]{1,0:T(8,128)(2,1)} %layer.1) | data formatting | bytes 262144
